TPU v7x, 32 devices: a whole 2x2x4 slice. The times are simulated.
32 devices in a mesh: grp: 2 (over y), sp: 8 (over z, core), tp: 2 (over x).
Axes of the slice: x: 2, y: 2, z: 4, core: 2. Of those that a mesh axis runs over, the one named last changes fastest.
Arguments:
- tokens: bfloat16 [12288, 2048], P(('grp', 'sp'), 'tp'), parts along dimension 0, may hold values from -4000 to 4000
- gain: float32 [2048], replicated, may hold values from 0.1 to 1.9
- w_query: bfloat16 [2048, 1024], P('sp', 'tp'), may hold values from -1 to 1
- w_key: bfloat16 [2048, 256], P('sp', 'tp'), may hold values from -1 to 1
- w_value: bfloat16 [2048, 256], P('sp', 'tp'), may hold values from -0.125 to 0.125
- w_input: bfloat16 [2048, 1024], P('sp', 'tp'), may hold values from -0.125 to 0.125
- w_bgate: bfloat16 [2048, 1024], P('sp', 'tp'), may hold values from -0.125 to 0.125
- w_cgate: bfloat16 [2048, 1024], P('sp', 'tp'), may hold values from -0.125 to 0.125
- w_attn_out: bfloat16 [1024, 2048], P('sp', 'tp'), may hold values from -2 to 2
- w_conv_out: bfloat16 [1024, 2048], P('sp', 'tp'), may hold values from -0.1875 to 0.1875
- sink_logit: float32 [16], P('tp'), may hold values from 0 to 5
- taps: float32 [3, 1024], P(None, 'tp'), may hold values from -3.5 to 3.5
- conv_bias: float32 [1024], P('tp'), may hold values from -4 to 4
- documents: int32 [12288], P(('grp', 'sp')), parts along dimension 0, may hold values from 0 to 3, never falling along the last dimension, each value on 1 to 3072 neighbouring positions
Outputs:
- mixed: bfloat16 [12288, 2048], P(('grp', 'sp'), 'tp'), parts along dimension 0
There are 2 independent parts, one for each index of `grp`. A program takes and returns all parts, laid end to end along the dimension named above; an argument that names none is the same for every part. Nothing has to cross between parts.
All inputs are finite; a program needn't handle non-finite values.
Results may differ from a plain program's by a relative error of at most 0.013.
The roundings to bfloat16 on the way count: a program that leaves them out, or rounds other values in their place, can miss the bound.
Values may be sent and summed in bfloat16 or wider, within the bound.
No kernel may reach another device: no remote copies, remote signals or barrier semaphores. Data moves between devices by JAX's collectives and lax.ppermute only.
A program may use at most 64 MiB of HBM per device.

v0:
```python
import jax
import jax.numpy as jnp
from jax import lax
from jax.experimental import pallas as pl
from jax.experimental.pallas import tpu as pltpu
from jax.sharding import PartitionSpec as P

HEAD_DIM = 64
WINDOW = 128


EPS = 1e-06
THETA = 500000.0


def extended(cells, sides, width):
    for axis, dim in sides:
        count = lax.axis_size(axis)
        ends = count - 1
        head = lax.slice_in_dim(cells, 0, width, axis=dim)
        tail = lax.slice_in_dim(cells, cells.shape[dim] - width, cells.shape[dim], axis=dim)
        cells = jnp.concatenate(
            [
                lax.ppermute(tail, axis, [(i, (i + 1) % count) for i in range(ends)]),
                cells,
                lax.ppermute(head, axis, [((i + 1) % count, i) for i in range(ends)]),
            ],
            axis=dim,
        )
    return cells


def rotate(proj, positions, heads):
    rows = proj.shape[0]
    size = proj.shape[1] // heads
    half = size // 2
    freq = jnp.power(THETA, -(jnp.arange(half, dtype=jnp.float32) * (2.0 / size)))
    angle = positions.astype(jnp.float32)[:, None] * freq[None, :]
    cosine = jnp.cos(angle)[:, None, :]
    sine = jnp.sin(angle)[:, None, :]
    shaped = proj.reshape(rows, heads, size)
    first = shaped[..., :half]
    second = shaped[..., half:]
    turned = jnp.concatenate(
        [first * cosine - second * sine, second * cosine + first * sine], axis=-1
    )
    return turned.reshape(rows, heads * size)


def sink_softmax(scores, allowed, sinks):
    masked = jnp.where(allowed, scores, -jnp.inf)
    top = jnp.maximum(jnp.max(masked, axis=-1, keepdims=True), sinks)
    expo = jnp.exp(masked - top)
    return expo / (jnp.sum(expo, axis=-1, keepdims=True) + jnp.exp(sinks - top))


CORES = 2
FEW_CHIPS = 8


def swap_parts(cells, axis):
    count = lax.axis_size(axis)
    return [cells] + [
        lax.ppermute(cells, axis, [(i, (i + d) % count) for i in range(count)])
        for d in range(1, count)
    ]


def shifted(cells, t, chips):
    perm = [(i, ((i // CORES + t) % chips) * CORES + i % CORES) for i in range(chips * CORES)]
    return lax.ppermute(cells, "sp", perm)


def join_kernel(*refs, spots, skip):
    out_ref = refs[-1]
    for ref, spot in zip(refs[skip:-1], spots):
        out_ref[spot : spot + ref.shape[0], :] = ref[...]


def joined(pieces, after=()):
    if pieces[0].shape[1] % 128 or any(p.shape[0] % 16 for p in pieces):
        return jnp.concatenate(pieces, axis=0)
    spots, rows = [], 0
    for piece in pieces:
        spots.append(rows)
        rows += piece.shape[0]
    vmem = pl.BlockSpec(memory_space=pltpu.VMEM)
    return pl.pallas_call(
        lambda *refs: join_kernel(*refs, spots=spots, skip=len(after)),
        out_shape=jax.ShapeDtypeStruct((rows, pieces[0].shape[1]), pieces[0].dtype),
        in_specs=[pl.BlockSpec(memory_space=pl.ANY)] * len(after) + [vmem] * len(pieces),
        out_specs=vmem,
        name="join_rows",
    )(*after, *pieces)


def spread(shard):
    chips = lax.axis_size("sp") // CORES
    piece = shard.shape[0] // lax.axis_size("grp")
    if chips > FEW_CHIPS:
        return []
    mine = lax.dynamic_slice_in_dim(shard, lax.axis_index("grp") * piece, piece, 0)
    out = []
    for t in range(1, chips):
        out.append(shifted(mine, t, chips))
    return out


def crossed(far, after=()):
    return swap_parts(joined(far, after), "grp") if far else []


def gathered(shard, parts, after=()):
    count = lax.axis_size("sp")
    if count // CORES > FEW_CHIPS:
        whole = lax.all_gather(shard, "sp", axis=0, tiled=True)
        return jnp.split(whole, 2)
    whole = joined([shard] + parts, after)
    return whole, lax.ppermute(whole, "sp", [(i, i ^ 1) for i in range(count)])


def relative_blocks():
    chips = lax.axis_size("sp") // CORES
    copies = lax.axis_size("grp")
    if chips > FEW_CHIPS:
        return [(s, j) for s in range(chips * CORES) for j in range(copies)]
    grp = lax.axis_index("grp")
    spot = lax.axis_index("sp")
    chip, core = spot // CORES, spot % CORES
    order = []
    for k in range(CORES):
        c = (core + k) % CORES
        order += [(chip * CORES + c, j) for j in range(copies)]
        for d in range(copies):
            for t in range(1, chips):
                order.append((((chip - t) % chips) * CORES + c, (grp - d) % copies))
    return order


def by_owner(feature, part, parts):
    return ((lax.axis_index("tp") - feature // part) % parts) * part + feature % part


def scale_kernel(at_ref, raw_at_ref, *refs, size):
    *tok_refs, gain_ref, out_ref, sq_ref = refs
    part = tok_refs[0].shape[1]
    for i in range(out_ref.shape[1] // size):
        factor = gain_ref[:, pl.ds(pl.multiple_of(raw_at_ref[i], size), size)]
        for p, tok_ref in enumerate(tok_refs):

            @pl.when(at_ref[i] // part == p)
            def _(tok_ref=tok_ref, factor=factor, i=i):
                cols = tok_ref[:, pl.ds(pl.multiple_of(at_ref[i] % part, size), size)]
                wide = cols.astype(jnp.float32) * factor
                out_ref[:, i * size : (i + 1) * size] = wide.astype(out_ref.dtype)

    total = None
    for tok_ref in tok_refs:
        for i in range(part // 128):
            cols = tok_ref[:, i * 128 : (i + 1) * 128].astype(jnp.float32)
            total = cols * cols if total is None else total + cols * cols
    sq_ref[...] = jnp.broadcast_to(jnp.sum(total, axis=1, keepdims=True), sq_ref.shape)


def pick_kernel(at_ref, *refs, size):
    *src_refs, out_ref = refs
    for i in range(out_ref.shape[1] // size):
        begin = 0
        for src_ref in src_refs:
            end = begin + src_ref.shape[1]

            @pl.when((at_ref[i] >= begin) & (at_ref[i] < end))
            def _(src_ref=src_ref, begin=begin, i=i):
                cols = pl.ds(pl.multiple_of(at_ref[i] - begin, size), size)
                out_ref[:, i * size : (i + 1) * size] = src_ref[:, cols]

            begin = end


def row_tile(rows):
    return rows // 4 if rows % 64 == 0 else rows


def scaled_blocks(toks, gain, at, raw_at, size):
    rows, width = toks[0].shape[0], gain.shape[0]
    tok = toks[0]
    if size % 128:
        wide = jnp.concatenate(toks, axis=1).astype(jnp.float32)
        out = [
            (
                lax.dynamic_slice_in_dim(wide, at[i], size, 1)
                * lax.dynamic_slice_in_dim(gain, raw_at[i], size, 0)[None, :]
            ).astype(tok.dtype)
            for i in range(width // size)
        ]
        return jnp.concatenate(out, axis=1), jnp.sum(wide * wide, axis=1, keepdims=True)
    tile = row_tile(rows)
    out, squares = pl.pallas_call(
        lambda *refs: scale_kernel(*refs, size=size),
        out_shape=(
            jax.ShapeDtypeStruct((rows, width), tok.dtype),
            jax.ShapeDtypeStruct((rows, 128), jnp.float32),
        ),
        grid_spec=pltpu.PrefetchScalarGridSpec(
            num_scalar_prefetch=2,
            grid=(rows // tile,),
            in_specs=[
                *(pl.BlockSpec((tile, t.shape[1]), lambda r, *_: (r, 0)) for t in toks),
                pl.BlockSpec((1, width), lambda r, *_: (0, 0)),
            ],
            out_specs=[
                pl.BlockSpec((tile, width), lambda r, *_: (r, 0)),
                pl.BlockSpec((tile, 128), lambda r, *_: (r, 0)),
            ],
        ),
        name="scale_blocks",
    )(at, raw_at, *toks, gain[None, :])
    return out, squares[:, :1]


def picked_blocks(srcs, at, size):
    rows, width = srcs[0].shape[0], sum(src.shape[1] for src in srcs)
    if size % 128:
        src = jnp.concatenate(srcs, axis=1)
        return jnp.concatenate(
            [lax.dynamic_slice_in_dim(src, at[i], size, 1) for i in range(width // size)], axis=1
        )
    tile = row_tile(rows)
    return pl.pallas_call(
        lambda *refs: pick_kernel(*refs, size=size),
        out_shape=jax.ShapeDtypeStruct((rows, width), srcs[0].dtype),
        grid_spec=pltpu.PrefetchScalarGridSpec(
            num_scalar_prefetch=1,
            grid=(rows // tile,),
            in_specs=[pl.BlockSpec((tile, src.shape[1]), lambda r, *_: (r, 0)) for src in srcs],
            out_specs=pl.BlockSpec((tile, width), lambda r, *_: (r, 0)),
        ),
        name="pick_blocks",
    )(at, *srcs)


def product(left, pair):
    cut = pair[0].shape[0]
    f32 = jnp.float32
    return jnp.dot(left[:, :cut], pair[0], preferred_element_type=f32) + jnp.dot(
        left[:, cut:], pair[1], preferred_element_type=f32
    )


def local(
    tokens,
    gain,
    w_query,
    w_key,
    w_value,
    w_input,
    w_bgate,
    w_cgate,
    w_attn_out,
    w_conv_out,
    sink_logit,
    taps,
    conv_bias,
    documents,
):
    f32 = jnp.float32
    bf16 = jnp.bfloat16
    rows, part = tokens.shape
    tp_count = lax.axis_size("tp")
    sp_count = lax.axis_size("sp")
    width = part * tp_count
    head_dim = HEAD_DIM
    q_local = w_query.shape[1] // head_dim
    kv_local = w_key.shape[1] // head_dim
    groups = q_local // kv_local
    copies = lax.axis_size("grp")
    toks = swap_parts(tokens, "tp")
    s_qkv = jnp.concatenate([w_query, w_key, w_value], axis=1)
    s_uc = jnp.concatenate([w_input, w_cgate], axis=1)
    s_out = jnp.concatenate([w_attn_out, w_conv_out], axis=0)
    far_qkv = spread(s_qkv)
    far_uc = spread(s_uc)
    far_b = spread(w_bgate)
    far_out = spread(s_out)
    y_qkv = crossed(far_qkv)
    y_uc = crossed(far_uc)
    g_qkv = gathered(s_qkv, y_qkv)
    order = relative_blocks()
    shard_rows = w_query.shape[0]
    size = shard_rows // copies
    raw_at = [shard * shard_rows + j * size for shard, j in order]
    at = jnp.stack([by_owner(f, part, tp_count) for f in raw_at]).astype(jnp.int32)
    raw_at = jnp.stack(raw_at).astype(jnp.int32)
    scaled, squares = scaled_blocks(toks, gain, at, raw_at, size)
    inv = lax.rsqrt(squares / width + EPS)
    qkv = product(scaled, g_qkv)
    q_width = w_query.shape[1]
    kv_width = w_key.shape[1]
    q_acc = qkv[:, :q_width]
    k_acc = qkv[:, q_width : q_width + kv_width]
    v_acc = qkv[:, q_width + kv_width :]
    positions = lax.axis_index("sp") * rows + jnp.arange(rows, dtype=jnp.int32)
    query = rotate(q_acc * inv, positions, q_local).astype(bf16)
    keys = rotate(k_acc * inv, positions, kv_local).astype(bf16)
    values = (v_acc * inv).astype(bf16)
    doc_row = documents.astype(f32).astype(bf16)[None, :]
    doc_ext = extended(doc_row, (("sp", 1),), WINDOW)[0].astype(f32)
    paired = jnp.concatenate([keys, values], axis=1)
    pair_ext = extended(paired, (("sp", 0),), WINDOW)
    g_uc = gathered(s_uc, y_uc, (paired,))
    y_b = crossed(far_b, (paired,))
    uc = product(scaled, g_uc)
    u_acc, c_acc = uc[:, : w_input.shape[1]], uc[:, w_input.shape[1] :]
    carried = (c_acc * inv * (u_acc * inv)).astype(bf16)
    carry_ext = extended(carried, (("sp", 0),), 1)
    key_width = kv_local * head_dim
    key_ext = pair_ext[:, :key_width].reshape(-1, kv_local, head_dim)
    val_ext = pair_ext[:, key_width:].reshape(-1, kv_local, head_dim)
    key_doc = doc_ext
    own_doc = documents.astype(f32)
    key_pos = positions[0] - WINDOW + jnp.arange(rows + 2 * WINDOW, dtype=jnp.int32)
    total = sp_count * rows
    sinks = sink_logit.reshape(kv_local, groups, 1, 1)
    block = rows // 2
    outputs = []
    for begin in range(0, rows, block):
        span = block + 2 * WINDOW
        q_block = query[begin : begin + block].reshape(block, kv_local, groups, head_dim)
        k_block = key_ext[begin : begin + span]
        v_block = val_ext[begin : begin + span]
        q_pos = positions[begin : begin + block]
        k_pos = key_pos[begin : begin + span]
        scores = jnp.einsum(
            "qhgd,khd->hgqk", q_block, k_block, preferred_element_type=f32
        ) * head_dim ** (-0.5)
        allowed = jnp.abs(q_pos[:, None] - k_pos[None, :]) <= WINDOW
        allowed = allowed & (
            own_doc[begin : begin + block, None] == key_doc[None, begin : begin + span]
        )
        allowed = allowed & (k_pos >= 0)[None, :] & (k_pos < total)[None, :]
        weight = sink_softmax(scores, allowed, sinks).astype(bf16)
        result = jnp.einsum("hgqk,khd->qhgd", weight, v_block, preferred_element_type=f32)
        outputs.append(result.astype(bf16).reshape(block, q_local * head_dim))
    attended = jnp.concatenate(outputs, axis=0)
    mixers = swap_parts(attended, "tp")
    y_out = crossed(far_out, (attended,))
    g_b = gathered(w_bgate, y_b, (attended,))
    bgate = product(scaled, g_b) * inv
    near_doc = doc_ext[WINDOW - 1 : WINDOW + rows + 1]
    conv = jnp.zeros((rows, carried.shape[1]), f32)
    for tap in range(3):
        same = (near_doc[tap : tap + rows] == near_doc[1 : rows + 1])[:, None]
        conv = conv + jnp.where(
            same, carry_ext[tap : tap + rows].astype(f32) * taps[tap][None, :], 0.0
        )
    convolved = (bgate * (conv + conv_bias[None, :])).astype(bf16)
    mixers += swap_parts(convolved, "tp")
    g_out = gathered(s_out, y_out, (convolved,))
    out_rows = w_attn_out.shape[0]
    q_part, c_part = attended.shape[1], convolved.shape[1]
    span = 2 * out_rows // copies
    places = []
    for shard, j in order:
        spot = j * span
        which, offset = spot // out_rows, spot % out_rows
        feature = shard * out_rows + offset
        places.append(
            jnp.where(
                which == 0,
                by_owner(feature, q_part, tp_count),
                q_part * tp_count + by_owner(feature, c_part, tp_count),
            )
        )
    picked = picked_blocks(mixers, jnp.stack(places).astype(jnp.int32), span)
    return product(picked, g_out).astype(bf16)


def solution(mesh):
    placed = (
        P(("grp", "sp"), "tp"),
        P(),
        P("sp", "tp"),
        P("sp", "tp"),
        P("sp", "tp"),
        P("sp", "tp"),
        P("sp", "tp"),
        P("sp", "tp"),
        P("sp", "tp"),
        P("sp", "tp"),
        P("tp"),
        P(None, "tp"),
        P("tp"),
        P(("grp", "sp")),
    )
    return jax.shard_map(
        local, mesh=mesh, in_specs=placed, out_specs=P(("grp", "sp"), "tp"), check_vma=False
    )
```

profile of v0, /device:TPU:0, one launch (start us, length us, event | category | flops | bytes accessed | tf_op | source)
XLA Modules:
  0.0 246.6 jit_solution(1976819392033191359)
XLA Ops:
  2.9 3.1 %collective-permute-start.1 = (bf16[128,768]{1,0:T(8,128)(2,1)S(1)}, bf16[128,768]{1,0:T(8,128)(2,1)S(1)}, u32[]{:S(2)}, u32[]{:S(2)}) collective-permute-start(bf16[128,768]{1,0:T(8,128)(2,1)S(1)} %constant_dynamic-slice_fusion.3), channel_id=1, source_target_pairs={{0,4},{2,6},{4,8},{6,10},{8,12},{10,14},{12,0},{14,2},{1,5},{3,7},... | collective-permute-start | bytes 589832 | tf_op jit(solution)/shard_map/ppermute | solution.py:71
  6.0 2.6 %collective-permute-start.2 = (bf16[128,768]{1,0:T(8,128)(2,1)S(1)}, bf16[128,768]{1,0:T(8,128)(2,1)S(1)}, u32[]{:S(2)}, u32[]{:S(2)}) collective-permute-start(bf16[128,768]{1,0:T(8,128)(2,1)S(1)} %constant_dynamic-slice_fusion.3), channel_id=1, source_target_pairs={{0,8},{2,10},{4,12},{6,14},{8,0},{10,2},{12,4},{14,6},{1,9},{3,11}... | collective-permute-start | bytes 589832 | tf_op jit(solution)/shard_map/ppermute | solution.py:71
  8.6 1.3 collective-permute-start.3
  9.9 4.0 %collective-permute-done.1.refs_0_ = bf16[128,768]{1,0:T(8,128)(2,1)S(1)} collective-permute-done((bf16[128,768]{1,0:T(8,128)(2,1)S(1)}, bf16[128,768]{1,0:T(8,128)(2,1)S(1)}, u32[]{:S(2)}, u32[]{:S(2)}) %collective-permute-start.1) | collective-permute-done | bytes 196640 | tf_op jit(solution)/shard_map/ppermute | solution.py:71
  13.9 7.6 %collective-permute-done.2.refs_1_ = bf16[128,768]{1,0:T(8,128)(2,1)S(1)} collective-permute-done((bf16[128,768]{1,0:T(8,128)(2,1)S(1)}, bf16[128,768]{1,0:T(8,128)(2,1)S(1)}, u32[]{:S(2)}, u32[]{:S(2)}) %collective-permute-start.2) | collective-permute-done | bytes 196640 | tf_op jit(solution)/shard_map/ppermute | solution.py:71
  22.8 2.0 join_rows.8.refs_1_
  24.8 1.5 collective-permute-start.4
  26.3 1.5 collective-permute-start
  27.8 12.4 %collective-permute-done.4.refs_2_ = bf16[384,768]{1,0:T(8,128)(2,1)S(1)} collective-permute-done((bf16[384,768]{1,0:T(8,128)(2,1)}, bf16[384,768]{1,0:T(8,128)(2,1)S(1)}, u32[]{:S(2)}, u32[]{:S(2)}) %collective-permute-start.4) | collective-permute-done | bytes 589856 | tf_op jit(solution)/shard_map/ppermute | solution.py:64
  41.0 2.6 %join_rows.9 = bf16[1024,768]{1,0:T(8,128)(2,1)} custom-call(bf16[256,768]{1,0:T(8,128)(2,1)} %copy-done.10, bf16[384,768]{1,0:T(8,128)(2,1)} %join_rows.8.refs_1_, bf16[384,768]{1,0:T(8,128)(2,1)} %copy-done.21), custom_call_target="tpu_custom_call" | custom-call | tf_op jit(solution)/shard_map/join_rows/pallas_call | solution.py:88
  43.7 4.2 %collective-permute-start.16 = (bf16[128,1024]{1,0:T(8,128)(2,1)S(1)}, bf16[128,1024]{1,0:T(8,128)(2,1)S(1)}, u32[]{:S(2)}, u32[]{:S(2)}) collective-permute-start(bf16[128,1024]{1,0:T(8,128)(2,1)S(1)} %constant_dynamic-slice_fusion.1), channel_id=1, source_target_pairs={{0,4},{2,6},{4,8},{6,10},{8,12},{10,14},{12,0},{14,2},{1,5},{3,7},... | collective-permute-start | bytes 786440 | tf_op jit(solution)/shard_map/ppermute | solution.py:71
  47.9 1.2 collective-permute-start.17
  49.1 1.2 collective-permute-start.18
  53.2 2.6 %collective-permute-done.16.refs_0_ = bf16[128,1024]{1,0:T(8,128)(2,1)S(1)} collective-permute-done((bf16[128,1024]{1,0:T(8,128)(2,1)S(1)}, bf16[128,1024]{1,0:T(8,128)(2,1)S(1)}, u32[]{:S(2)}, u32[]{:S(2)}) %collective-permute-start.16) | collective-permute-done | bytes 262176 | tf_op jit(solution)/shard_map/ppermute | solution.py:71
  55.9 1.2 collective-permute-start.11
  57.1 10.0 %collective-permute-done.17.refs_1_ = bf16[128,1024]{1,0:T(8,128)(2,1)S(1)} collective-permute-done((bf16[128,1024]{1,0:T(8,128)(2,1)S(1)}, bf16[128,1024]{1,0:T(8,128)(2,1)S(1)}, u32[]{:S(2)}, u32[]{:S(2)}) %collective-permute-start.17) | collective-permute-done | bytes 262176 | tf_op jit(solution)/shard_map/ppermute | solution.py:71
  67.8 2.1 join_rows.12.refs_2_
  69.9 1.5 collective-permute-start.19
  71.4 7.1 %scale_blocks.1 = (bf16[768,2048]{1,0:T(8,128)(2,1)}, f32[768,128]{1,0:T(8,128)}) custom-call(s32[16]{0:T(128)} %stack.186.refs_0_, s32[16]{0:T(128)} %stack.203.refs_1_, bf16[768,1024]{1,0:T(8,128)(2,1)} %refs_2_.1, bf16[768,1024]{1,0:T(8,128)(2,1)} %collective-permute-done.refs_3_, f32[1,2048]{1,0:T(1,128)} %bitcast.131), custom_call_target="tpu_custom_call" | custom-call | tf_op jit(solution)/shard_map/scale_blocks/pallas_call | solution.py:198
  78.5 1.2 rsqrt_reduce_fusion
  79.7 3.4 %fusion.17 = f32[768,768]{1,0:T(8,128)S(1)} fusion(bf16[1024,768]{1,0:T(8,128)(2,1)} %collective-permute-done.5, bf16[768,2048]{1,0:T(8,128)(2,1)} %get-tuple-element.7), kind=kOutput, calls=%fused_computation.30 | convolution fusion | flops 1207959552 | bytes 5505024 | tf_op jit(solution)/shard_map/dot_general | solution.py:245
  83.1 1.4 convolution_add_fusion.1
  84.5 1.4 copy-done.4
  87.4 2.1 collective-permute-done.19.refs_3_
  89.5 3.0 %join_rows.13 = bf16[1024,1024]{1,0:T(8,128)(2,1)} custom-call(bf16[768,256]{1,0:T(8,128)(2,1)} %pad_maximum_fusion.3.refs_0_, bf16[256,1024]{1,0:T(8,128)(2,1)} %copy-done.6, bf16[384,1024]{1,0:T(8,128)(2,1)} %join_rows.12.refs_2_, bf16[384,1024]{1,0:T(8,128)(2,1)} %collective-permute-done.19.refs_3_), custom_call_target="tpu_custom_call" | custom-call | tf_op jit(solution)/shard_map/join_rows/pallas_call | solution.py:88
  92.5 1.3 collective-permute-start.8
  93.8 3.0 %collective-permute-start.7 = (bf16[1,128]{1,0:T(2,128)(2,1)S(1)}, bf16[1,128]{1,0:T(2,128)(2,1)S(1)}, u32[]{:S(2)}, u32[]{:S(2)}) collective-permute-start(bf16[1,128]{1,0:T(2,128)(2,1)S(1)} %get-tuple-element.51), channel_id=1, source_target_pairs={{0,2},{2,4},{4,6},{6,8},{8,10},{10,12},{12,14},{1,3},{3,5},{5,7},{... | collective-permute-start | bytes 776 | tf_op jit(solution)/shard_map/ppermute | solution.py:24
  98.2 9.9 %collective-permute-start.13 = (bf16[128,512]{1,0:T(8,128)(2,1)S(1)}, bf16[128,512]{1,0:T(8,128)(2,1)S(1)}, u32[]{:S(2)}, u32[]{:S(2)}) collective-permute-start(bf16[128,512]{1,0:T(8,128)(2,1)S(1)} %copy-done.39), channel_id=1, source_target_pairs={{0,12},{2,14},{4,0},{6,2},{8,4},{10,6},{12,8},{14,10},{1,13},{3,15... | collective-permute-start | bytes 393224 | tf_op jit(solution)/shard_map/ppermute | solution.py:71
  108.9 1.3 collective-permute-start.6
  110.2 1.5 collective-permute-start.9
  111.7 1.4 fusion.28
  113.7 1.8 join_rows.10.refs_2_
  115.5 1.5 collective-permute-start.14
  120.4 4.0 %fusion.13 = f32[768,1024]{1,0:T(8,128)S(1)} fusion(bf16[1024,1024]{1,0:T(8,128)(2,1)} %collective-permute-done.20, bf16[768,2048]{1,0:T(8,128)(2,1)} %get-tuple-element.7), kind=kOutput, calls=%fused_computation.26 | convolution fusion | flops 1610612736 | bytes 6815744 | tf_op jit(solution)/shard_map/dot_general | solution.py:245
  124.4 1.8 convolution_add_fusion
  126.2 1.2 slice_multiply_fusion.2
  128.0 1.1 subtract_convert_fusion
  129.3 1.4 fusion.2
  130.7 1.6 fusion
  132.4 1.3 fusion.3
  133.8 1.6 fusion.1
  135.5 2.6 %fusion.11 = bf16[2,64,4,384]{3,1,2,0:T(8,128)(2,1)S(1)} fusion(bf16[640,2,64,1]{0,2,3,1:T(8,128)(2,1)S(1)} %bitcast.129, f32[2,640,384,4]{2,1,3,0:T(8,128)S(1)} %get-tuple-element.58, f32[2,4,384]{2,1,0:T(4,128)S(1)} %exponential_add_fusion, f32[2,4,384]{2,1,0:T(4,128)S(1)} %get-tuple-element.54, pred[384,640]{0,1:T(8,128)(4,1)S(1)} %fusion.26), kind=kOutput, calls=%fused_computation.24 | convolution fusion | flops 261685248 | bytes 8691712 | tf_op jit(solution)/shard_map/hgqk,khd->qhgd/dot_general | solution.py:342
  138.1 2.8 %fusion.12 = bf16[2,64,4,384]{3,1,2,0:T(8,128)(2,1)S(1)} fusion(bf16[640,2,64,1]{0,2,3,1:T(8,128)(2,1)S(1)} %bitcast.130, f32[2,640,384,4]{2,1,3,0:T(8,128)S(1)} %get-tuple-element.56, f32[2,4,384]{2,1,0:T(4,128)S(1)} %get-tuple-element.53, f32[2,4,384]{2,1,0:T(4,128)S(1)} %broadcast_maximum_fusion.1, pred[384,640]{0,1:T(8,128)(4,1)S(1)} %copy-done.1), kind=kOutput, calls=%fused_computation.25 | convolution fusion | flops 261685248 | bytes 8691712 | tf_op jit(solution)/shard_map/hgqk,khd->qhgd/dot_general | solution.py:342
  142.3 2.3 join_rows.11
  144.6 1.8 collective-permute-start.15
  146.5 2.2 collective-permute-start.24
  148.7 1.8 collective-permute-start.25
  150.5 2.5 %collective-permute-start.26 = (bf16[128,1024]{1,0:T(8,128)(2,1)S(1)}, bf16[128,1024]{1,0:T(8,128)(2,1)S(1)}, u32[]{:S(2)}, u32[]{:S(2)}) collective-permute-start(bf16[128,1024]{1,0:T(8,128)(2,1)S(1)} %constant_dynamic-slice_fusion), channel_id=1, source_target_pairs={{0,12},{2,14},{4,0},{6,2},{8,4},{10,6},{12,8},{14,10},{1,13},{3,15... | collective-permute-start | bytes 786440 | tf_op jit(solution)/shard_map/ppermute | solution.py:71
  153.1 1.3 collective-permute-start.22
  154.4 3.3 %collective-permute-done.24.refs_1_ = bf16[128,1024]{1,0:T(8,128)(2,1)S(1)} collective-permute-done((bf16[128,1024]{1,0:T(8,128)(2,1)S(1)}, bf16[128,1024]{1,0:T(8,128)(2,1)S(1)}, u32[]{:S(2)}, u32[]{:S(2)}) %collective-permute-start.24) | collective-permute-done | bytes 262176 | tf_op jit(solution)/shard_map/ppermute | solution.py:71
  157.7 1.3 collective-permute-start.21
  159.0 9.3 %collective-permute-done.25.refs_2_ = bf16[128,1024]{1,0:T(8,128)(2,1)S(1)} collective-permute-done((bf16[128,1024]{1,0:T(8,128)(2,1)S(1)}, bf16[128,1024]{1,0:T(8,128)(2,1)S(1)}, u32[]{:S(2)}, u32[]{:S(2)}) %collective-permute-start.25) | collective-permute-done | bytes 262176 | tf_op jit(solution)/shard_map/ppermute | solution.py:71
  169.6 2.0 join_rows.14.refs_2_
  172.2 2.9 %fusion.15 = f32[768,512]{1,0:T(8,128)S(1)} fusion(bf16[1024,512]{1,0:T(8,128)(2,1)} %collective-permute-done.15, bf16[768,2048]{1,0:T(8,128)(2,1)} %get-tuple-element.7), kind=kOutput, calls=%fused_computation.28 | convolution fusion | flops 805306368 | bytes 4194304 | tf_op jit(solution)/shard_map/dot_general | solution.py:245
  175.2 3.1 %multiply_convert_fusion.refs_3_.refs_0_ = bf16[768,512]{1,0:T(8,128)(2,1)} fusion(bf16[768,512]{1,0:T(8,128)(2,1)S(1)} %copy-done.15, f32[768,512]{1,0:T(8,128)S(1)} %fusion.15, bf16[1,512]{1,0:T(2,128)(2,1)S(1)} %collective-permute-done.22, bf16[1,512]{1,0:T(2,128)(2,1)S(1)} %collective-permute-done.21, f32[512]{0:T(512)S(1)} %copy-done.45, ...), kind=kOutput, calls=%fused_computation.22 | convolution fusion | flops 813957120 | bytes 5786624 | tf_op jit(solution)/shard_map/dot_general | solution.py:245
  178.3 12.7 %collective-permute-done.27.refs_3_ = bf16[384,1024]{1,0:T(8,128)(2,1)S(1)} collective-permute-done((bf16[384,1024]{1,0:T(8,128)(2,1)}, bf16[384,1024]{1,0:T(8,128)(2,1)S(1)}, u32[]{:S(2)}, u32[]{:S(2)}) %collective-permute-start.27) | collective-permute-done | bytes 786464 | tf_op jit(solution)/shard_map/ppermute | solution.py:64
  191.8 3.0 %join_rows.15 = bf16[1024,1024]{1,0:T(8,128)(2,1)} custom-call(bf16[768,512]{1,0:T(8,128)(2,1)} %multiply_convert_fusion.refs_3_.refs_0_, bf16[256,1024]{1,0:T(8,128)(2,1)} %copy-done.7, bf16[384,1024]{1,0:T(8,128)(2,1)} %join_rows.14.refs_2_, bf16[384,1024]{1,0:T(8,128)(2,1)} %copy-done.18), custom_call_target="tpu_custom_call" | custom-call | tf_op jit(solution)/shard_map/join_rows/pallas_call | solution.py:88
  194.8 1.2 collective-permute-start.28
  196.0 1.5 collective-permute-start.10
  198.7 17.7 %collective-permute-done.10.refs_2_ = bf16[768,512]{1,0:T(8,128)(2,1)S(1)} collective-permute-done((bf16[768,512]{1,0:T(8,128)(2,1)S(1)}, bf16[768,512]{1,0:T(8,128)(2,1)S(1)}, u32[]{:S(2)}, u32[]{:S(2)}) %collective-permute-start.10) | collective-permute-done | bytes 786464 | tf_op jit(solution)/shard_map/ppermute | solution.py:64
  216.4 15.9 %collective-permute-done.23.refs_4_ = bf16[768,512]{1,0:T(8,128)(2,1)S(1)} collective-permute-done((bf16[768,512]{1,0:T(8,128)(2,1)S(1)}, bf16[768,512]{1,0:T(8,128)(2,1)S(1)}, u32[]{:S(2)}, u32[]{:S(2)}) %collective-permute-start.23) | collective-permute-done | bytes 786464 | tf_op jit(solution)/shard_map/ppermute | solution.py:64
  233.2 6.4 %pick_blocks.1 = bf16[768,2048]{1,0:T(8,128)(2,1)} custom-call(s32[16]{0:T(128)} %stack.169.refs_0_, bf16[768,512]{1,0:T(8,128)(2,1)} %pad_maximum_fusion.2.refs_0_.refs_1_, bf16[768,512]{1,0:T(8,128)(2,1)} %copy-done.16, bf16[768,512]{1,0:T(8,128)(2,1)} %multiply_convert_fusion.refs_3_.refs_0_, bf16[768,512]{1,0:T(8,128)(2,1)} %copy-done.17), custom_call_target="tpu_custom_call" | custom-call | tf_op jit(solution)/shard_map/pick_blocks/pallas_call | solution.py:229
  239.6 4.0 %fusion.6 = f32[768,1024]{1,0:T(8,128)S(1)} fusion(bf16[1024,1024]{1,0:T(8,128)(2,1)} %collective-permute-done.28, bf16[768,2048]{1,0:T(8,128)(2,1)} %pick_blocks.1), kind=kOutput, calls=%fused_computation.14 | convolution fusion | flops 1610612736 | bytes 6815744 | tf_op jit(solution)/shard_map/dot_general | solution.py:245
  243.6 2.9 %add_convert_fusion = bf16[768,1024]{1,0:T(8,128)(2,1)} fusion(f32[768,1024]{1,0:T(8,128)S(1)} %fusion.6, bf16[1024,1024]{1,0:T(8,128)(2,1)S(1)} %copy-done.8, bf16[768,2048]{1,0:T(8,128)(2,1)S(1)} %copy-done.3), kind=kOutput, calls=%fused_computation.12 | convolution fusion | flops 1612185600 | bytes 8388608 | tf_op jit(solution)/shard_map/dot_general | solution.py:245
  (169 shorter events, 22.3 us)
Async XLA Ops:
  0.0 26.3 %copy-start.11 = (bf16[768,1024]{1,0:T(8,128)(2,1)S(1)}, bf16[768,1024]{1,0:T(8,128)(2,1)}, u32[]{:S(2)}) copy-start(bf16[768,1024]{1,0:T(8,128)(2,1)} %refs_2_.1) | copy-start | bytes 4718596
  2.8 37.3 %copy-start.10 = (bf16[256,768]{1,0:T(8,128)(2,1)}, bf16[256,768]{1,0:T(8,128)(2,1)S(1)}, u32[]{:S(2)}) copy-start(bf16[256,768]{1,0:T(8,128)(2,1)S(1)} %constant_dynamic-update-slice_fusion.refs_0_) | copy-start | bytes 1179652
  2.9 40.7 %copy-start.26 = (bf16[256,512]{1,0:T(8,128)(2,1)S(1)}, bf16[256,512]{1,0:T(8,128)(2,1)}, u32[]{:S(2)}) copy-start(bf16[256,512]{1,0:T(8,128)(2,1)} %param.19) | copy-start | bytes 786436
  2.9 11.0 %collective-permute-start.1 = (bf16[128,768]{1,0:T(8,128)(2,1)S(1)}, bf16[128,768]{1,0:T(8,128)(2,1)S(1)}, u32[]{:S(2)}, u32[]{:S(2)}) collective-permute-start(bf16[128,768]{1,0:T(8,128)(2,1)S(1)} %constant_dynamic-slice_fusion.3), channel_id=1, source_target_pairs={{0,4},{2,6},{4,8},{6,10},{8,12},{10,14},{12,0},{14,2},{1,5},{3,7},... | collective-permute-start | bytes 589832 | tf_op jit(solution)/shard_map/ppermute | solution.py:71
  6.0 15.5 %collective-permute-start.2 = (bf16[128,768]{1,0:T(8,128)(2,1)S(1)}, bf16[128,768]{1,0:T(8,128)(2,1)S(1)}, u32[]{:S(2)}, u32[]{:S(2)}) collective-permute-start(bf16[128,768]{1,0:T(8,128)(2,1)S(1)} %constant_dynamic-slice_fusion.3), channel_id=1, source_target_pairs={{0,8},{2,10},{4,12},{6,14},{8,0},{10,2},{12,4},{14,6},{1,9},{3,11}... | collective-permute-start | bytes 589832 | tf_op jit(solution)/shard_map/ppermute | solution.py:71
  8.6 12.9 %collective-permute-start.3 = (bf16[128,768]{1,0:T(8,128)(2,1)S(1)}, bf16[128,768]{1,0:T(8,128)(2,1)S(1)}, u32[]{:S(2)}, u32[]{:S(2)}) collective-permute-start(bf16[128,768]{1,0:T(8,128)(2,1)S(1)} %constant_dynamic-slice_fusion.3), channel_id=1, source_target_pairs={{0,12},{2,14},{4,0},{6,2},{8,4},{10,6},{12,8},{14,10},{1,13},{3,15... | collective-permute-start | bytes 589832 | tf_op jit(solution)/shard_map/ppermute | solution.py:71
  13.9 7.6 %copy-start.32 = (bf16[128,768]{1,0:T(8,128)(2,1)}, bf16[128,768]{1,0:T(8,128)(2,1)S(1)}, u32[]{:S(2)}) copy-start(bf16[128,768]{1,0:T(8,128)(2,1)S(1)} %collective-permute-done.1.refs_0_) | copy-start | bytes 589828
  24.8 18.8 %copy-start.27 = (bf16[256,512]{1,0:T(8,128)(2,1)S(1)}, bf16[256,512]{1,0:T(8,128)(2,1)}, u32[]{:S(2)}) copy-start(bf16[256,512]{1,0:T(8,128)(2,1)} %param.21) | copy-start | bytes 786436
  24.8 25.5 %copy-start.22 = (bf16[256,512]{1,0:T(8,128)(2,1)S(1)}, bf16[256,512]{1,0:T(8,128)(2,1)}, u32[]{:S(2)}) copy-start(bf16[256,512]{1,0:T(8,128)(2,1)} %refs_1_.1) | copy-start | bytes 786436
  24.8 26.2 %copy-start.41 = (s32[768]{0:T(1024)S(1)}, s32[768]{0:T(1024)}, u32[]{:S(2)}) copy-start(s32[768]{0:T(1024)} %param.27) | copy-start | bytes 9220
  24.8 15.4 %collective-permute-start.4 = (bf16[384,768]{1,0:T(8,128)(2,1)}, bf16[384,768]{1,0:T(8,128)(2,1)S(1)}, u32[]{:S(2)}, u32[]{:S(2)}) collective-permute-start(bf16[384,768]{1,0:T(8,128)(2,1)} %join_rows.8.refs_1_), channel_id=1, source_target_pairs={{0,16},{16,0},{1,17},{17,1},{2,18},{18,2},{3,19},{19,3},{4,20},{20... | collective-permute-start | bytes 1769480 | tf_op jit(solution)/shard_map/ppermute | solution.py:64
  26.3 45.1 %collective-permute-start = (bf16[768,1024]{1,0:T(8,128)(2,1)S(1)}, bf16[768,1024]{1,0:T(8,128)(2,1)}, u32[]{:S(2)}, u32[]{:S(2)}) collective-permute-start(bf16[768,1024]{1,0:T(8,128)(2,1)S(1)} %copy-done.11), channel_id=1, source_target_pairs={{0,1},{1,0},{2,3},{3,2},{4,5},{5,4},{6,7},{7,6},{8,9},{9,8},{10,11... | collective-permute-start | bytes 4718600 | tf_op jit(solution)/shard_map/ppermute | solution.py:64
  43.6 36.1 %collective-permute-start.5 = (bf16[1024,768]{1,0:T(8,128)(2,1)}, bf16[1024,768]{1,0:T(8,128)(2,1)}, u32[]{:S(2)}, u32[]{:S(2)}) collective-permute-start(bf16[1024,768]{1,0:T(8,128)(2,1)} %join_rows.9), channel_id=1, source_target_pairs={{0,2},{2,0},{4,6},{6,4},{8,10},{10,8},{12,14},{14,12},{1,3},{3,1},... | collective-permute-start | bytes 4718600 | tf_op jit(solution)/shard_map/ppermute | solution.py:119
  43.7 34.8 %copy-start.6 = (bf16[256,1024]{1,0:T(8,128)(2,1)}, bf16[256,1024]{1,0:T(8,128)(2,1)S(1)}, u32[]{:S(2)}) copy-start(bf16[256,1024]{1,0:T(8,128)(2,1)S(1)} %constant_dynamic-update-slice_fusion.3.refs_1_) | copy-start | bytes 1572868
  43.7 12.1 %collective-permute-start.16 = (bf16[128,1024]{1,0:T(8,128)(2,1)S(1)}, bf16[128,1024]{1,0:T(8,128)(2,1)S(1)}, u32[]{:S(2)}, u32[]{:S(2)}) collective-permute-start(bf16[128,1024]{1,0:T(8,128)(2,1)S(1)} %constant_dynamic-slice_fusion.1), channel_id=1, source_target_pairs={{0,4},{2,6},{4,8},{6,10},{8,12},{10,14},{12,0},{14,2},{1,5},{3,7},... | collective-permute-start | bytes 786440 | tf_op jit(solution)/shard_map/ppermute | solution.py:71
  47.9 19.2 %collective-permute-start.17 = (bf16[128,1024]{1,0:T(8,128)(2,1)S(1)}, bf16[128,1024]{1,0:T(8,128)(2,1)S(1)}, u32[]{:S(2)}, u32[]{:S(2)}) collective-permute-start(bf16[128,1024]{1,0:T(8,128)(2,1)S(1)} %constant_dynamic-slice_fusion.1), channel_id=1, source_target_pairs={{0,8},{2,10},{4,12},{6,14},{8,0},{10,2},{12,4},{14,6},{1,9},{3,11}... | collective-permute-start | bytes 786440 | tf_op jit(solution)/shard_map/ppermute | solution.py:71
  49.1 18.0 %collective-permute-start.18 = (bf16[128,1024]{1,0:T(8,128)(2,1)S(1)}, bf16[128,1024]{1,0:T(8,128)(2,1)}, u32[]{:S(2)}, u32[]{:S(2)}) collective-permute-start(bf16[128,1024]{1,0:T(8,128)(2,1)S(1)} %constant_dynamic-slice_fusion.1), channel_id=1, source_target_pairs={{0,12},{2,14},{4,0},{6,2},{8,4},{10,6},{12,8},{14,10},{1,13},{3,15... | collective-permute-start | bytes 786440 | tf_op jit(solution)/shard_map/ppermute | solution.py:71
  53.2 33.1 %copy-start.14 = (f32[768,32]{0,1:T(8,128)}, f32[768,32]{0,1:T(8,128)S(1)}, u32[]{:S(2)}) copy-start(f32[768,32]{0,1:T(8,128)S(1)} %get-tuple-element.36) | copy-start | bytes 294916
  55.9 11.2 %copy-start.30 = (bf16[128,1024]{1,0:T(8,128)(2,1)}, bf16[128,1024]{1,0:T(8,128)(2,1)S(1)}, u32[]{:S(2)}) copy-start(bf16[128,1024]{1,0:T(8,128)(2,1)S(1)} %collective-permute-done.16.refs_0_) | copy-start | bytes 786436
  55.9 54.3 %collective-permute-start.11 = (bf16[128,512]{1,0:T(8,128)(2,1)}, bf16[128,512]{1,0:T(8,128)(2,1)S(1)}, u32[]{:S(2)}, u32[]{:S(2)}) collective-permute-start(bf16[128,512]{1,0:T(8,128)(2,1)} %constant_dynamic-slice_fusion.2), channel_id=1, source_target_pairs={{0,4},{2,6},{4,8},{6,10},{8,12},{10,14},{12,0},{14,2},{1,5},{3,7},... | collective-permute-start | bytes 393224 | tf_op jit(solution)/shard_map/ppermute | solution.py:71
  67.1 46.0 %collective-permute-start.12 = (bf16[128,512]{1,0:T(8,128)(2,1)}, bf16[128,512]{1,0:T(8,128)(2,1)}, u32[]{:S(2)}, u32[]{:S(2)}) collective-permute-start(bf16[128,512]{1,0:T(8,128)(2,1)} %constant_dynamic-slice_fusion.2), channel_id=1, source_target_pairs={{0,8},{2,10},{4,12},{6,14},{8,0},{10,2},{12,4},{14,6},{1,9},{3,11}... | collective-permute-start | bytes 393224 | tf_op jit(solution)/shard_map/ppermute | solution.py:71
  69.9 19.6 %collective-permute-start.19 = (bf16[384,1024]{1,0:T(8,128)(2,1)}, bf16[384,1024]{1,0:T(8,128)(2,1)}, u32[]{:S(2)}, u32[]{:S(2)}) collective-permute-start(bf16[384,1024]{1,0:T(8,128)(2,1)} %join_rows.12.refs_2_), channel_id=1, source_target_pairs={{0,16},{16,0},{1,17},{17,1},{2,18},{18,2},{3,19},{19,3},{4,20},{20... | collective-permute-start | bytes 2359304 | tf_op jit(solution)/shard_map/ppermute | solution.py:64
  79.7 3.4 %copy-start.12 = (bf16[1024,768]{1,0:T(8,128)(2,1)S(1)}, bf16[1024,768]{1,0:T(8,128)(2,1)}, u32[]{:S(2)}) copy-start(bf16[1024,768]{1,0:T(8,128)(2,1)} %join_rows.9) | copy-start | bytes 4718596
  79.7 3.4 %copy-start.42 = (bf16[768,2048]{1,0:T(8,128)(2,1)S(1)}, bf16[768,2048]{1,0:T(8,128)(2,1)}, u32[]{:S(2)}) copy-start(bf16[768,2048]{1,0:T(8,128)(2,1)} %get-tuple-element.7) | copy-start | bytes 9437188
  87.4 10.8 %copy-start.46 = (f32[8]{0:T(128)S(1)}, f32[8]{0:T(128)}, u32[]{:S(2)}) copy-start(f32[8]{0:T(128)} %param.24) | copy-start | bytes 100
  87.4 10.8 %copy-start.39 = (bf16[128,512]{1,0:T(8,128)(2,1)S(1)}, bf16[128,512]{1,0:T(8,128)(2,1)}, u32[]{:S(2)}) copy-start(bf16[128,512]{1,0:T(8,128)(2,1)} %constant_dynamic-slice_fusion.2) | copy-start | bytes 393220
  92.5 27.8 %collective-permute-start.20 = (bf16[1024,1024]{1,0:T(8,128)(2,1)}, bf16[1024,1024]{1,0:T(8,128)(2,1)}, u32[]{:S(2)}, u32[]{:S(2)}) collective-permute-start(bf16[1024,1024]{1,0:T(8,128)(2,1)} %join_rows.13), channel_id=1, source_target_pairs={{0,2},{2,0},{4,6},{6,4},{8,10},{10,8},{12,14},{14,12},{1,3},{3,1},... | collective-permute-start | bytes 6291464 | tf_op jit(solution)/shard_map/ppermute | solution.py:119
  92.5 5.7 %collective-permute-start.8 = (bf16[1,128]{1,0:T(2,128)(2,1)S(1)}, bf16[1,128]{1,0:T(2,128)(2,1)S(1)}, u32[]{:S(2)}, u32[]{:S(2)}) collective-permute-start(bf16[1,128]{1,0:T(2,128)(2,1)S(1)} %get-tuple-element.52), channel_id=1, source_target_pairs={{2,0},{4,2},{6,4},{8,6},{10,8},{12,10},{14,12},{3,1},{5,3},{7,5},{... | collective-permute-start | bytes 776 | tf_op jit(solution)/shard_map/ppermute | solution.py:26
  93.8 14.3 %collective-permute-start.7 = (bf16[1,128]{1,0:T(2,128)(2,1)S(1)}, bf16[1,128]{1,0:T(2,128)(2,1)S(1)}, u32[]{:S(2)}, u32[]{:S(2)}) collective-permute-start(bf16[1,128]{1,0:T(2,128)(2,1)S(1)} %get-tuple-element.51), channel_id=1, source_target_pairs={{0,2},{2,4},{4,6},{6,8},{8,10},{10,12},{12,14},{1,3},{3,5},{5,7},{... | collective-permute-start | bytes 776 | tf_op jit(solution)/shard_map/ppermute | solution.py:24
  98.2 14.9 %collective-permute-start.13 = (bf16[128,512]{1,0:T(8,128)(2,1)S(1)}, bf16[128,512]{1,0:T(8,128)(2,1)S(1)}, u32[]{:S(2)}, u32[]{:S(2)}) collective-permute-start(bf16[128,512]{1,0:T(8,128)(2,1)S(1)} %copy-done.39), channel_id=1, source_target_pairs={{0,12},{2,14},{4,0},{6,2},{8,4},{10,6},{12,8},{14,10},{1,13},{3,15... | collective-permute-start | bytes 393224 | tf_op jit(solution)/shard_map/ppermute | solution.py:71
  108.9 8.1 %collective-permute-start.6 = (bf16[128,256]{1,0:T(8,128)(2,1)S(1)}, bf16[128,256]{1,0:T(8,128)(2,1)S(1)}, u32[]{:S(2)}, u32[]{:S(2)}) collective-permute-start(bf16[128,256]{1,0:T(8,128)(2,1)S(1)} %get-tuple-element.30), channel_id=1, source_target_pairs={{0,2},{2,4},{4,6},{6,8},{8,10},{10,12},{12,14},{1,3},{3,5},{5,7},{... | collective-permute-start | bytes 196616 | tf_op jit(solution)/shard_map/ppermute | solution.py:24
  110.2 2.9 %copy-start.37 = (bf16[128,512]{1,0:T(8,128)(2,1)}, bf16[128,512]{1,0:T(8,128)(2,1)S(1)}, u32[]{:S(2)}) copy-start(bf16[128,512]{1,0:T(8,128)(2,1)S(1)} %collective-permute-done.11.refs_1_) | copy-start | bytes 393220
  110.2 6.8 %collective-permute-start.9 = (bf16[128,256]{1,0:T(8,128)(2,1)S(1)}, bf16[128,256]{1,0:T(8,128)(2,1)S(1)}, u32[]{:S(2)}, u32[]{:S(2)}) collective-permute-start(bf16[128,256]{1,0:T(8,128)(2,1)S(1)} %get-tuple-element.31), channel_id=1, source_target_pairs={{2,0},{4,2},{6,4},{8,6},{10,8},{12,10},{14,12},{3,1},{5,3},{7,5},{... | collective-permute-start | bytes 196616 | tf_op jit(solution)/shard_map/ppermute | solution.py:26
  115.5 26.8 %collective-permute-start.14 = (bf16[384,512]{1,0:T(8,128)(2,1)}, bf16[384,512]{1,0:T(8,128)(2,1)}, u32[]{:S(2)}, u32[]{:S(2)}) collective-permute-start(bf16[384,512]{1,0:T(8,128)(2,1)} %join_rows.10.refs_2_), channel_id=1, source_target_pairs={{0,16},{16,0},{1,17},{17,1},{2,18},{18,2},{3,19},{19,3},{4,20},{20... | collective-permute-start | bytes 1179656 | tf_op jit(solution)/shard_map/ppermute | solution.py:64
  120.3 4.0 %copy-start.9 = (bf16[1024,1024]{1,0:T(8,128)(2,1)S(1)}, bf16[1024,1024]{1,0:T(8,128)(2,1)}, u32[]{:S(2)}) copy-start(bf16[1024,1024]{1,0:T(8,128)(2,1)} %join_rows.13) | copy-start | bytes 6291460
  120.3 4.0 %copy-start.43 = (bf16[768,2048]{1,0:T(8,128)(2,1)S(1)}, bf16[768,2048]{1,0:T(8,128)(2,1)}, u32[]{:S(2)}) copy-start(bf16[768,2048]{1,0:T(8,128)(2,1)} %get-tuple-element.7) | copy-start | bytes 9437188
  124.4 1.9 copy-start.5
  130.7 1.6 copy-start.19
  133.8 1.7 copy-start.35
  135.5 2.6 %copy-start.36 = (bf16[640,128]{0,1:T(8,128)(2,1)S(1)}, bf16[640,128]{0,1:T(8,128)(2,1)}, u32[]{:S(2)}) copy-start(bf16[640,128]{0,1:T(8,128)(2,1)} %copy.31) | copy-start | bytes 491524
  141.3 5.1 %copy-start.28 = (bf16[128,1024]{1,0:T(8,128)(2,1)S(1)}, bf16[128,1024]{1,0:T(8,128)(2,1)}, u32[]{:S(2)}) copy-start(bf16[128,1024]{1,0:T(8,128)(2,1)} %param.22) | copy-start | bytes 786436
  142.3 4.2 %copy-start.29 = (bf16[128,1024]{1,0:T(8,128)(2,1)S(1)}, bf16[128,1024]{1,0:T(8,128)(2,1)}, u32[]{:S(2)}) copy-start(bf16[128,1024]{1,0:T(8,128)(2,1)} %param.23) | copy-start | bytes 786436
  142.3 10.7 %copy-start.40 = (f32[3,512]{1,0:T(4,128)S(1)}, f32[3,512]{1,0:T(4,128)}, u32[]{:S(2)}) copy-start(f32[3,512]{1,0:T(4,128)} %param.25) | copy-start | bytes 18436
  142.3 10.8 %copy-start.15 = (bf16[768,512]{1,0:T(8,128)(2,1)S(1)}, bf16[768,512]{1,0:T(8,128)(2,1)}, u32[]{:S(2)}) copy-start(bf16[768,512]{1,0:T(8,128)(2,1)} %get-tuple-element.50) | copy-start | bytes 2359300
  144.6 27.6 %collective-permute-start.15 = (bf16[1024,512]{1,0:T(8,128)(2,1)}, bf16[1024,512]{1,0:T(8,128)(2,1)}, u32[]{:S(2)}, u32[]{:S(2)}) collective-permute-start(bf16[1024,512]{1,0:T(8,128)(2,1)} %join_rows.11), channel_id=1, source_target_pairs={{0,2},{2,0},{4,6},{6,4},{8,10},{10,8},{12,14},{14,12},{1,3},{3,1},... | collective-permute-start | bytes 3145736 | tf_op jit(solution)/shard_map/ppermute | solution.py:119
  146.5 28.7 %copy-start.7 = (bf16[256,1024]{1,0:T(8,128)(2,1)}, bf16[256,1024]{1,0:T(8,128)(2,1)S(1)}, u32[]{:S(2)}) copy-start(bf16[256,1024]{1,0:T(8,128)(2,1)S(1)} %constant_dynamic-update-slice_fusion.5.refs_1_) | copy-start | bytes 1572868
  146.5 11.2 %collective-permute-start.24 = (bf16[128,1024]{1,0:T(8,128)(2,1)S(1)}, bf16[128,1024]{1,0:T(8,128)(2,1)S(1)}, u32[]{:S(2)}, u32[]{:S(2)}) collective-permute-start(bf16[128,1024]{1,0:T(8,128)(2,1)S(1)} %constant_dynamic-slice_fusion), channel_id=1, source_target_pairs={{0,4},{2,6},{4,8},{6,10},{8,12},{10,14},{12,0},{14,2},{1,5},{3,7},... | collective-permute-start | bytes 786440 | tf_op jit(solution)/shard_map/ppermute | solution.py:71
  148.7 19.5 %collective-permute-start.25 = (bf16[128,1024]{1,0:T(8,128)(2,1)S(1)}, bf16[128,1024]{1,0:T(8,128)(2,1)S(1)}, u32[]{:S(2)}, u32[]{:S(2)}) collective-permute-start(bf16[128,1024]{1,0:T(8,128)(2,1)S(1)} %constant_dynamic-slice_fusion), channel_id=1, source_target_pairs={{0,8},{2,10},{4,12},{6,14},{8,0},{10,2},{12,4},{14,6},{1,9},{3,11}... | collective-permute-start | bytes 786440 | tf_op jit(solution)/shard_map/ppermute | solution.py:71
  150.5 17.8 %collective-permute-start.26 = (bf16[128,1024]{1,0:T(8,128)(2,1)S(1)}, bf16[128,1024]{1,0:T(8,128)(2,1)S(1)}, u32[]{:S(2)}, u32[]{:S(2)}) collective-permute-start(bf16[128,1024]{1,0:T(8,128)(2,1)S(1)} %constant_dynamic-slice_fusion), channel_id=1, source_target_pairs={{0,12},{2,14},{4,0},{6,2},{8,4},{10,6},{12,8},{14,10},{1,13},{3,15... | collective-permute-start | bytes 786440 | tf_op jit(solution)/shard_map/ppermute | solution.py:71
  153.1 22.1 %collective-permute-start.22 = (bf16[1,512]{1,0:T(2,128)(2,1)S(1)}, bf16[1,512]{1,0:T(2,128)(2,1)S(1)}, u32[]{:S(2)}, u32[]{:S(2)}) collective-permute-start(bf16[1,512]{1,0:T(2,128)(2,1)S(1)} %get-tuple-element.19), channel_id=1, source_target_pairs={{2,0},{4,2},{6,4},{8,6},{10,8},{12,10},{14,12},{3,1},{5,3},{7,5},{... | collective-permute-start | bytes 3080 | tf_op jit(solution)/shard_map/ppermute | solution.py:26
  157.7 10.6 %copy-start.23 = (bf16[128,1024]{1,0:T(8,128)(2,1)}, bf16[128,1024]{1,0:T(8,128)(2,1)S(1)}, u32[]{:S(2)}) copy-start(bf16[128,1024]{1,0:T(8,128)(2,1)S(1)} %collective-permute-done.24.refs_1_) | copy-start | bytes 786436
  157.7 17.5 %collective-permute-start.21 = (bf16[1,512]{1,0:T(2,128)(2,1)S(1)}, bf16[1,512]{1,0:T(2,128)(2,1)S(1)}, u32[]{:S(2)}, u32[]{:S(2)}) collective-permute-start(bf16[1,512]{1,0:T(2,128)(2,1)S(1)} %get-tuple-element.18), channel_id=1, source_target_pairs={{0,2},{2,4},{4,6},{6,8},{8,10},{10,12},{12,14},{1,3},{3,5},{5,7},{... | collective-permute-start | bytes 3080 | tf_op jit(solution)/shard_map/ppermute | solution.py:24
  171.7 3.5 %copy-start.13 = (bf16[1024,512]{1,0:T(8,128)(2,1)S(1)}, bf16[1024,512]{1,0:T(8,128)(2,1)}, u32[]{:S(2)}) copy-start(bf16[1024,512]{1,0:T(8,128)(2,1)} %join_rows.11) | copy-start | bytes 3145732
  171.7 3.5 %copy-start.44 = (bf16[768,2048]{1,0:T(8,128)(2,1)S(1)}, bf16[768,2048]{1,0:T(8,128)(2,1)}, u32[]{:S(2)}) copy-start(bf16[768,2048]{1,0:T(8,128)(2,1)} %get-tuple-element.7) | copy-start | bytes 9437188
  171.7 3.5 %copy-start.45 = (f32[512]{0:T(512)S(1)}, f32[512]{0:T(512)}, u32[]{:S(2)}) copy-start(f32[512]{0:T(512)} %param.26) | copy-start | bytes 6148
  171.7 19.3 %collective-permute-start.27 = (bf16[384,1024]{1,0:T(8,128)(2,1)}, bf16[384,1024]{1,0:T(8,128)(2,1)S(1)}, u32[]{:S(2)}, u32[]{:S(2)}) collective-permute-start(bf16[384,1024]{1,0:T(8,128)(2,1)} %join_rows.14.refs_2_), channel_id=1, source_target_pairs={{0,16},{16,0},{1,17},{17,1},{2,18},{18,2},{3,19},{19,3},{4,20},{20... | collective-permute-start | bytes 2359304 | tf_op jit(solution)/shard_map/ppermute | solution.py:64
  178.3 17.7 %copy-start = (bf16[768,512]{1,0:T(8,128)(2,1)S(1)}, bf16[768,512]{1,0:T(8,128)(2,1)}, u32[]{:S(2)}) copy-start(bf16[768,512]{1,0:T(8,128)(2,1)} %pad_maximum_fusion.2.refs_0_.refs_1_) | copy-start | bytes 2359300
  178.3 19.2 %copy-start.2 = (bf16[768,512]{1,0:T(8,128)(2,1)S(1)}, bf16[768,512]{1,0:T(8,128)(2,1)}, u32[]{:S(2)}) copy-start(bf16[768,512]{1,0:T(8,128)(2,1)} %multiply_convert_fusion.refs_3_.refs_0_) | copy-start | bytes 2359300
  194.8 44.8 %collective-permute-start.28 = (bf16[1024,1024]{1,0:T(8,128)(2,1)}, bf16[1024,1024]{1,0:T(8,128)(2,1)}, u32[]{:S(2)}, u32[]{:S(2)}) collective-permute-start(bf16[1024,1024]{1,0:T(8,128)(2,1)} %join_rows.15), channel_id=1, source_target_pairs={{0,2},{2,0},{4,6},{6,4},{8,10},{10,8},{12,14},{14,12},{1,3},{3,1},... | collective-permute-start | bytes 6291464 | tf_op jit(solution)/shard_map/ppermute | solution.py:119
  196.0 20.4 %collective-permute-start.10 = (bf16[768,512]{1,0:T(8,128)(2,1)S(1)}, bf16[768,512]{1,0:T(8,128)(2,1)S(1)}, u32[]{:S(2)}, u32[]{:S(2)}) collective-permute-start(bf16[768,512]{1,0:T(8,128)(2,1)S(1)} %copy-done), channel_id=1, source_target_pairs={{0,1},{1,0},{2,3},{3,2},{4,5},{5,4},{6,7},{7,6},{8,9},{9,8},{10,11... | collective-permute-start | bytes 2359304 | tf_op jit(solution)/shard_map/ppermute | solution.py:64
  197.5 34.8 %collective-permute-start.23 = (bf16[768,512]{1,0:T(8,128)(2,1)S(1)}, bf16[768,512]{1,0:T(8,128)(2,1)S(1)}, u32[]{:S(2)}, u32[]{:S(2)}) collective-permute-start(bf16[768,512]{1,0:T(8,128)(2,1)S(1)} %copy-done.2), channel_id=1, source_target_pairs={{0,1},{1,0},{2,3},{3,2},{4,5},{5,4},{6,7},{7,6},{8,9},{9,8},{10,11... | collective-permute-start | bytes 2359304 | tf_op jit(solution)/shard_map/ppermute | solution.py:64
  216.4 15.9 %copy-start.16 = (bf16[768,512]{1,0:T(8,128)(2,1)}, bf16[768,512]{1,0:T(8,128)(2,1)S(1)}, u32[]{:S(2)}) copy-start(bf16[768,512]{1,0:T(8,128)(2,1)S(1)} %collective-permute-done.10.refs_2_) | copy-start | bytes 2359300
  239.6 4.0 %copy-start.3 = (bf16[768,2048]{1,0:T(8,128)(2,1)S(1)}, bf16[768,2048]{1,0:T(8,128)(2,1)}, u32[]{:S(2)}) copy-start(bf16[768,2048]{1,0:T(8,128)(2,1)} %pick_blocks.1) | copy-start | bytes 9437188
  239.6 4.0 %copy-start.8 = (bf16[1024,1024]{1,0:T(8,128)(2,1)S(1)}, bf16[1024,1024]{1,0:T(8,128)(2,1)}, u32[]{:S(2)}) copy-start(bf16[1024,1024]{1,0:T(8,128)(2,1)} %join_rows.15) | copy-start | bytes 6291460
  (12 other events, 10.7 us)
where the time goes:
time: 250 us; the launch traced here: 247 us
  waiting for transfers between devices  97.5 us (39%)
  starting transfers between devices  52.4 us (21%)
  Pallas kernels  32.4 us (13%)
  matrix products  31.6 us (13%)
  local copies, waits for them, and re-layouts  18.8 us (8%)
  other arithmetic  11.9 us (5%)
    ppermute x7, waiting for transfers between devices, swap_parts(): lax.ppermute(cells, axis, [(i, (i + d) % count) for i in range(count)])  60.8 us
    ppermute x12, waiting for transfers between devices, shifted(): return lax.ppermute(cells, 'sp', perm)  36.7 us
    ppermute x12, starting transfers between devices, shifted(): return lax.ppermute(cells, 'sp', perm)  31.2 us
    pallas_call x8, Pallas kernels, joined(): pl.pallas_call(lambda *refs: join_kernel(*refs, spots=spots, skip=len(aft...  18.9 us
    dot_general x4, matrix products, product(): jnp.dot(left[:, cut:], pair[1], preferred_element_type=f32)  14.4 us
    unnamed x98, local copies, waits for them, and re-layouts  10.2 us
    dot_general x4, matrix products, product(): jnp.dot(left[:, :cut], pair[0], preferred_element_type=f32)  9.25 us
    ppermute x7, starting transfers between devices, swap_parts(): lax.ppermute(cells, axis, [(i, (i + d) % count) for i in range(count)])  8.56 us
  transfers between devices with their start and end apart: 29, of which 11 were waited for; matrix products, arithmetic and copies ran while one was open for 18% of the time, Pallas kernels for 10%

commit v1 on v0

--- a/solution.py
+++ b/solution.py
@@ -308,7 +308,9 @@
     paired = jnp.concatenate([keys, values], axis=1)
     pair_ext = extended(paired, (("sp", 0),), WINDOW)
     g_uc = gathered(s_uc, y_uc, (paired,))
-    y_b = crossed(far_b, (paired,))
+    y_b = crossed(far_b, (inv,))
+    g_b = gathered(w_bgate, y_b, (paired,))
+    y_out = crossed(far_out, (paired,))
     uc = product(scaled, g_uc)
     u_acc, c_acc = uc[:, : w_input.shape[1]], uc[:, w_input.shape[1] :]
     carried = (c_acc * inv * (u_acc * inv)).astype(bf16)
@@ -343,8 +345,7 @@
         outputs.append(result.astype(bf16).reshape(block, q_local * head_dim))
     attended = jnp.concatenate(outputs, axis=0)
     mixers = swap_parts(attended, "tp")
-    y_out = crossed(far_out, (attended,))
-    g_b = gathered(w_bgate, y_b, (attended,))
+    g_out = gathered(s_out, y_out, (attended,))
     bgate = product(scaled, g_b) * inv
     near_doc = doc_ext[WINDOW - 1 : WINDOW + rows + 1]
     conv = jnp.zeros((rows, carried.shape[1]), f32)
@@ -355,7 +356,6 @@
         )
     convolved = (bgate * (conv + conv_bias[None, :])).astype(bf16)
     mixers += swap_parts(convolved, "tp")
-    g_out = gathered(s_out, y_out, (convolved,))
     out_rows = w_attn_out.shape[0]
     q_part, c_part = attended.shape[1], convolved.shape[1]
     span = 2 * out_rows // copies

time: 250 us -> 229 us (0.916)
  waiting for transfers between devices: 97.5 us -> 73.8 us
  starting transfers between devices: 52.4 us -> 57 us
    ppermute x12, waiting for transfers between devices: 36.7 us -> 15.7 us  [shifted(): return lax.ppermute(cells, 'sp', perm)]
    ppermute x4, starting transfers between devices: 3 us -> 12.4 us  [gathered(): lax.ppermute(whole, 'sp', [(i, i ^ 1) for i in range(count)])]
    ppermute x12, starting transfers between devices: 31.2 us -> 27.2 us  [shifted(): return lax.ppermute(cells, 'sp', perm)]
    dot_general x2, matrix products: 5.34 us -> 8.28 us  [local(): jnp.einsum('hgqk,khd->qhgd', weight, v_block, preferred_element_type=f32)]
    ppermute x7, waiting for transfers between devices: 60.8 us -> 58.1 us  [swap_parts(): lax.ppermute(cells, axis, [(i, (i + d) % count) for i in range(count)])]
    unnamed x98 -> x78, local copies, waits for them, and re-layouts: 10.2 us -> 8.33 us
  transfers between devices with their start and end apart: 29 -> 29, of which waited for: 11 -> 11; matrix products, arithmetic and copies ran while one was open for 18% -> 21% of each run, Pallas kernels for 10% -> 12%
where the time goes in v1:
time: 229 us; the launch traced here: 228 us
  waiting for transfers between devices  73.8 us (32%)
  starting transfers between devices  57 us (25%)
  matrix products  34 us (15%)
  Pallas kernels  32.4 us (14%)
  local copies, waits for them, and re-layouts  18.9 us (8%)
  other arithmetic  10 us (4%)
    ppermute x7, waiting for transfers between devices, swap_parts(): lax.ppermute(cells, axis, [(i, (i + d) % count) for i in range(count)])  58.1 us
    ppermute x12, starting transfers between devices, shifted(): return lax.ppermute(cells, 'sp', perm)  27.2 us
    pallas_call x8, Pallas kernels, joined(): pl.pallas_call(lambda *refs: join_kernel(*refs, spots=spots, skip=len(aft...  18.9 us
    ppermute x12, waiting for transfers between devices, shifted(): return lax.ppermute(cells, 'sp', perm)  15.7 us
    dot_general x4, matrix products, product(): jnp.dot(left[:, cut:], pair[1], preferred_element_type=f32)  13.6 us
    ppermute x4, starting transfers between devices, gathered(): lax.ppermute(whole, 'sp', [(i, i ^ 1) for i in range(count)])  12.4 us
    dot_general x4, matrix products, product(): jnp.dot(left[:, :cut], pair[0], preferred_element_type=f32)  9.4 us
    unnamed x78, local copies, waits for them, and re-layouts  8.33 us
  transfers between devices with their start and end apart: 29, of which 11 were waited for; matrix products, arithmetic and copies ran while one was open for 21% of the time, Pallas kernels for 12%

profile of v1, /device:TPU:0, one launch (start us, length us, event | category | flops | bytes accessed | tf_op | source)
XLA Modules:
  0.0 227.7 jit_solution(12546419625848336971)
XLA Ops:
  0.0 1.1 constant_dynamic-update-slice_fusion.2
  2.9 3.1 %collective-permute-start.1 = (bf16[128,768]{1,0:T(8,128)(2,1)S(1)}, bf16[128,768]{1,0:T(8,128)(2,1)S(1)}, u32[]{:S(2)}, u32[]{:S(2)}) collective-permute-start(bf16[128,768]{1,0:T(8,128)(2,1)S(1)} %constant_dynamic-slice_fusion.3), channel_id=1, source_target_pairs={{0,4},{2,6},{4,8},{6,10},{8,12},{10,14},{12,0},{14,2},{1,5},{3,7},... | collective-permute-start | bytes 589832 | tf_op jit(solution)/shard_map/ppermute | solution.py:71
  6.0 2.6 %collective-permute-start.2 = (bf16[128,768]{1,0:T(8,128)(2,1)S(1)}, bf16[128,768]{1,0:T(8,128)(2,1)S(1)}, u32[]{:S(2)}, u32[]{:S(2)}) collective-permute-start(bf16[128,768]{1,0:T(8,128)(2,1)S(1)} %constant_dynamic-slice_fusion.3), channel_id=1, source_target_pairs={{0,8},{2,10},{4,12},{6,14},{8,0},{10,2},{12,4},{14,6},{1,9},{3,11}... | collective-permute-start | bytes 589832 | tf_op jit(solution)/shard_map/ppermute | solution.py:71
  8.6 1.3 collective-permute-start.3
  9.9 4.0 %collective-permute-done.1.refs_0_ = bf16[128,768]{1,0:T(8,128)(2,1)S(1)} collective-permute-done((bf16[128,768]{1,0:T(8,128)(2,1)S(1)}, bf16[128,768]{1,0:T(8,128)(2,1)S(1)}, u32[]{:S(2)}, u32[]{:S(2)}) %collective-permute-start.1) | collective-permute-done | bytes 196640 | tf_op jit(solution)/shard_map/ppermute | solution.py:71
  13.9 7.6 %collective-permute-done.2.refs_1_ = bf16[128,768]{1,0:T(8,128)(2,1)S(1)} collective-permute-done((bf16[128,768]{1,0:T(8,128)(2,1)S(1)}, bf16[128,768]{1,0:T(8,128)(2,1)S(1)}, u32[]{:S(2)}, u32[]{:S(2)}) %collective-permute-start.2) | collective-permute-done | bytes 196640 | tf_op jit(solution)/shard_map/ppermute | solution.py:71
  22.8 2.0 join_rows.8.refs_1_
  24.8 1.5 collective-permute-start.4
  26.3 1.5 collective-permute-start
  28.0 4.1 %collective-permute-start.16 = (bf16[128,1024]{1,0:T(8,128)(2,1)S(1)}, bf16[128,1024]{1,0:T(8,128)(2,1)}, u32[]{:S(2)}, u32[]{:S(2)}) collective-permute-start(bf16[128,1024]{1,0:T(8,128)(2,1)S(1)} %constant_dynamic-slice_fusion.1), channel_id=1, source_target_pairs={{0,4},{2,6},{4,8},{6,10},{8,12},{10,14},{12,0},{14,2},{1,5},{3,7},... | collective-permute-start | bytes 786440 | tf_op jit(solution)/shard_map/ppermute | solution.py:71
  32.0 2.3 %collective-permute-start.17 = (bf16[128,1024]{1,0:T(8,128)(2,1)S(1)}, bf16[128,1024]{1,0:T(8,128)(2,1)}, u32[]{:S(2)}, u32[]{:S(2)}) collective-permute-start(bf16[128,1024]{1,0:T(8,128)(2,1)S(1)} %constant_dynamic-slice_fusion.1), channel_id=1, source_target_pairs={{0,8},{2,10},{4,12},{6,14},{8,0},{10,2},{12,4},{14,6},{1,9},{3,11}... | collective-permute-start | bytes 786440 | tf_op jit(solution)/shard_map/ppermute | solution.py:71
  34.5 5.8 %collective-permute-done.4.refs_2_ = bf16[384,768]{1,0:T(8,128)(2,1)} collective-permute-done((bf16[384,768]{1,0:T(8,128)(2,1)}, bf16[384,768]{1,0:T(8,128)(2,1)}, u32[]{:S(2)}, u32[]{:S(2)}) %collective-permute-start.4) | collective-permute-done | bytes 589856 | tf_op jit(solution)/shard_map/ppermute | solution.py:64
  40.3 2.6 %join_rows.9 = bf16[1024,768]{1,0:T(8,128)(2,1)} custom-call(bf16[256,768]{1,0:T(8,128)(2,1)} %copy-done.8, bf16[384,768]{1,0:T(8,128)(2,1)} %join_rows.8.refs_1_, bf16[384,768]{1,0:T(8,128)(2,1)} %collective-permute-done.4.refs_2_), custom_call_target="tpu_custom_call" | custom-call | tf_op jit(solution)/shard_map/join_rows/pallas_call | solution.py:88
  43.7 1.0 constant_dynamic-update-slice_fusion.5.refs_1_
  48.4 4.2 %collective-permute-start.11 = (bf16[128,512]{1,0:T(8,128)(2,1)}, bf16[128,512]{1,0:T(8,128)(2,1)}, u32[]{:S(2)}, u32[]{:S(2)}) collective-permute-start(bf16[128,512]{1,0:T(8,128)(2,1)} %constant_dynamic-slice_fusion.2), channel_id=1, source_target_pairs={{0,4},{2,6},{4,8},{6,10},{8,12},{10,14},{12,0},{14,2},{1,5},{3,7},... | collective-permute-start | bytes 393224 | tf_op jit(solution)/shard_map/ppermute | solution.py:71
  52.6 1.2 collective-permute-start.12
  53.8 1.3 collective-permute-start.8
  55.1 2.1 join_rows.12.refs_2_
  57.2 5.1 %collective-permute-done.refs_3_ = bf16[768,1024]{1,0:T(8,128)(2,1)} collective-permute-done((bf16[768,1024]{1,0:T(8,128)(2,1)S(1)}, bf16[768,1024]{1,0:T(8,128)(2,1)}, u32[]{:S(2)}, u32[]{:S(2)}) %collective-permute-start) | collective-permute-done | bytes 1572896 | tf_op jit(solution)/shard_map/ppermute | solution.py:64
  62.4 1.3 collective-permute-start.7
  63.7 7.1 %scale_blocks.1 = (bf16[768,2048]{1,0:T(8,128)(2,1)}, f32[768,128]{1,0:T(8,128)}) custom-call(s32[16]{0:T(128)} %stack.186.refs_0_, s32[16]{0:T(128)} %stack.203.refs_1_, bf16[768,1024]{1,0:T(8,128)(2,1)} %refs_2_.1, bf16[768,1024]{1,0:T(8,128)(2,1)} %collective-permute-done.refs_3_, f32[1,2048]{1,0:T(1,128)} %bitcast.131), custom_call_target="tpu_custom_call" | custom-call | tf_op jit(solution)/shard_map/scale_blocks/pallas_call | solution.py:198
  70.7 1.8 add_rsqrt_fusion
  73.1 3.4 %fusion.17 = f32[768,768]{1,0:T(8,128)S(1)} fusion(bf16[1024,768]{1,0:T(8,128)(2,1)} %collective-permute-done.5, bf16[768,2048]{1,0:T(8,128)(2,1)} %get-tuple-element.7), kind=kOutput, calls=%fused_computation.30 | convolution fusion | flops 1207959552 | bytes 5505024 | tf_op jit(solution)/shard_map/dot_general | solution.py:245
  76.6 1.4 convolution_add_fusion.1
  78.2 1.2 copy-done.23
  80.6 8.5 %collective-permute-done.19.refs_3_ = bf16[384,1024]{1,0:T(8,128)(2,1)S(1)} collective-permute-done((bf16[384,1024]{1,0:T(8,128)(2,1)S(1)}, bf16[384,1024]{1,0:T(8,128)(2,1)S(1)}, u32[]{:S(2)}, u32[]{:S(2)}) %collective-permute-start.19) | collective-permute-done | bytes 786464 | tf_op jit(solution)/shard_map/ppermute | solution.py:64
  90.0 3.0 %join_rows.13 = bf16[1024,1024]{1,0:T(8,128)(2,1)} custom-call(bf16[768,256]{1,0:T(8,128)(2,1)} %pad_maximum_fusion.3.refs_0_, bf16[256,1024]{1,0:T(8,128)(2,1)} %copy-done.4, bf16[384,1024]{1,0:T(8,128)(2,1)} %join_rows.12.refs_2_, bf16[384,1024]{1,0:T(8,128)(2,1)} %copy-done.14), custom_call_target="tpu_custom_call" | custom-call | tf_op jit(solution)/shard_map/join_rows/pallas_call | solution.py:88
  93.0 3.7 %collective-permute-start.20 = (bf16[1024,1024]{1,0:T(8,128)(2,1)}, bf16[1024,1024]{1,0:T(8,128)(2,1)}, u32[]{:S(2)}, u32[]{:S(2)}) collective-permute-start(bf16[1024,1024]{1,0:T(8,128)(2,1)} %join_rows.13), channel_id=1, source_target_pairs={{0,2},{2,0},{4,6},{6,4},{8,10},{10,8},{12,14},{14,12},{1,3},{3,1},... | collective-permute-start | bytes 6291464 | tf_op jit(solution)/shard_map/ppermute | solution.py:119
  96.9 1.8 collective-permute-start.13
  98.7 2.0 collective-permute-start.24
  100.8 2.1 collective-permute-start.25
  102.9 2.3 %collective-permute-start.26 = (bf16[128,1024]{1,0:T(8,128)(2,1)S(1)}, bf16[128,1024]{1,0:T(8,128)(2,1)S(1)}, u32[]{:S(2)}, u32[]{:S(2)}) collective-permute-start(bf16[128,1024]{1,0:T(8,128)(2,1)S(1)} %constant_dynamic-slice_fusion), channel_id=1, source_target_pairs={{0,12},{2,14},{4,0},{6,2},{8,4},{10,6},{12,8},{14,10},{1,13},{3,15... | collective-permute-start | bytes 786440 | tf_op jit(solution)/shard_map/ppermute | solution.py:71
  106.3 1.8 join_rows.10.refs_2_
  109.9 2.6 %collective-permute-done.24.refs_1_ = bf16[128,1024]{1,0:T(8,128)(2,1)S(1)} collective-permute-done((bf16[128,1024]{1,0:T(8,128)(2,1)S(1)}, bf16[128,1024]{1,0:T(8,128)(2,1)S(1)}, u32[]{:S(2)}, u32[]{:S(2)}) %collective-permute-start.24) | collective-permute-done | bytes 262176 | tf_op jit(solution)/shard_map/ppermute | solution.py:71
  112.5 1.3 collective-permute-start.6
  113.8 4.9 %collective-permute-done.14.refs_3_ = bf16[384,512]{1,0:T(8,128)(2,1)S(1)} collective-permute-done((bf16[384,512]{1,0:T(8,128)(2,1)}, bf16[384,512]{1,0:T(8,128)(2,1)S(1)}, u32[]{:S(2)}, u32[]{:S(2)}) %collective-permute-start.14) | collective-permute-done | bytes 393248 | tf_op jit(solution)/shard_map/ppermute | solution.py:64
  118.7 1.5 collective-permute-start.9
  120.3 2.2 join_rows.11
  122.5 1.1 collective-permute-done.25.refs_2_
  123.6 5.6 %collective-permute-start.15 = (bf16[1024,512]{1,0:T(8,128)(2,1)}, bf16[1024,512]{1,0:T(8,128)(2,1)}, u32[]{:S(2)}, u32[]{:S(2)}) collective-permute-start(bf16[1024,512]{1,0:T(8,128)(2,1)} %join_rows.11), channel_id=1, source_target_pairs={{0,2},{2,0},{4,6},{6,4},{8,10},{10,8},{12,14},{14,12},{1,3},{3,1},... | collective-permute-start | bytes 3145736 | tf_op jit(solution)/shard_map/ppermute | solution.py:119
  129.9 2.0 join_rows.14.refs_2_
  131.9 1.7 collective-permute-start.27
  135.7 4.0 %fusion.13 = f32[768,1024]{1,0:T(8,128)S(1)} fusion(bf16[1024,1024]{1,0:T(8,128)(2,1)} %collective-permute-done.20, bf16[768,2048]{1,0:T(8,128)(2,1)} %get-tuple-element.7), kind=kOutput, calls=%fused_computation.26 | convolution fusion | flops 1610612736 | bytes 6815744 | tf_op jit(solution)/shard_map/dot_general | solution.py:245
  139.7 1.8 convolution_add_fusion
  141.8 1.3 collective-permute-start.22
  143.1 3.3 %collective-permute-start.21 = (bf16[1,512]{1,0:T(2,128)(2,1)S(1)}, bf16[1,512]{1,0:T(2,128)(2,1)S(1)}, u32[]{:S(2)}, u32[]{:S(2)}) collective-permute-start(bf16[1,512]{1,0:T(2,128)(2,1)S(1)} %get-tuple-element.18), channel_id=1, source_target_pairs={{0,2},{2,4},{4,6},{6,8},{8,10},{10,12},{12,14},{1,3},{3,5},{5,7},{... | collective-permute-start | bytes 3080 | tf_op jit(solution)/shard_map/ppermute | solution.py:24
  146.4 2.2 fusion.15
  148.7 3.2 %multiply_convert_fusion = (bf16[768,512]{1,0:T(8,128)(2,1)S(1)}, f32[768,512]{1,0:T(8,128)}) fusion(bf16[768,512]{1,0:T(8,128)(2,1)S(1)} %fusion.10, f32[768,512]{1,0:T(8,128)S(1)} %fusion.15, bf16[1,512]{1,0:T(2,128)(2,1)S(1)} %collective-permute-done.22, bf16[1,512]{1,0:T(2,128)(2,1)S(1)} %collective-permute-done.21, f32[512]{0:T(512)S(1)} %copy-done.35, ...), kind=kOutput, calls=%fused_computation.22 | convolution fusion | flops 814350336 | bytes 8932352 | tf_op jit(solution)/shard_map/dot_general | solution.py:245
  151.9 2.2 copy.33
  154.4 1.4 fusion.2
  155.9 1.6 fusion
  157.5 1.4 copy-done
  158.9 1.3 fusion.3
  160.3 1.7 fusion.1
  162.1 2.8 %fusion.11 = bf16[2,64,4,384]{3,1,2,0:T(8,128)(2,1)S(1)} fusion(bf16[640,2,64,1]{0,2,3,1:T(8,128)(2,1)S(1)} %bitcast.130, f32[2,640,384,4]{2,1,3,0:T(8,128)S(1)} %get-tuple-element.60, f32[2,4,384]{2,1,0:T(4,128)S(1)} %exponential_add_fusion, f32[2,4,384]{2,1,0:T(4,128)S(1)} %get-tuple-element.56, pred[384,640]{0,1:T(8,128)(4,1)S(1)} %fusion.26), kind=kOutput, calls=%fused_computation.24 | convolution fusion | flops 261685248 | bytes 8691712 | tf_op jit(solution)/shard_map/hgqk,khd->qhgd/dot_general | solution.py:344
  165.1 5.5 %fusion.12 = bf16[2,64,4,384]{3,1,2,0:T(8,128)(2,1)S(1)} fusion(bf16[640,2,64,1]{0,2,3,1:T(8,128)(2,1)S(1)} %bitcast.129, f32[2,640,384,4]{2,1,3,0:T(8,128)} %copy-done, f32[2,4,384]{2,1,0:T(4,128)S(1)} %get-tuple-element.55, f32[2,4,384]{2,1,0:T(4,128)S(1)} %broadcast_maximum_fusion.1, pred[384,640]{0,1:T(8,128)(4,1)S(1)} %fusion.28), kind=kOutput, calls=%fused_computation.25 | convolution fusion | flops 261685248 | bytes 8691712 | tf_op jit(solution)/shard_map/hgqk,khd->qhgd/dot_general | solution.py:344
  171.7 3.1 %join_rows.15 = bf16[1024,1024]{1,0:T(8,128)(2,1)} custom-call(bf16[768,512]{1,0:T(8,128)(2,1)} %pad_maximum_fusion.2.refs_1_.refs_0_, bf16[256,1024]{1,0:T(8,128)(2,1)} %copy-done.5, bf16[384,1024]{1,0:T(8,128)(2,1)} %join_rows.14.refs_2_, bf16[384,1024]{1,0:T(8,128)(2,1)} %collective-permute-done.27.refs_3_), custom_call_target="tpu_custom_call" | custom-call | tf_op jit(solution)/shard_map/join_rows/pallas_call | solution.py:88
  174.8 3.1 %collective-permute-start.28 = (bf16[1024,1024]{1,0:T(8,128)(2,1)}, bf16[1024,1024]{1,0:T(8,128)(2,1)}, u32[]{:S(2)}, u32[]{:S(2)}) collective-permute-start(bf16[1024,1024]{1,0:T(8,128)(2,1)} %join_rows.15), channel_id=1, source_target_pairs={{0,2},{2,0},{4,6},{6,4},{8,10},{10,8},{12,14},{14,12},{1,3},{3,1},... | collective-permute-start | bytes 6291464 | tf_op jit(solution)/shard_map/ppermute | solution.py:119
  177.9 1.4 collective-permute-start.10
  180.5 17.7 %collective-permute-done.10.refs_2_ = bf16[768,512]{1,0:T(8,128)(2,1)S(1)} collective-permute-done((bf16[768,512]{1,0:T(8,128)(2,1)S(1)}, bf16[768,512]{1,0:T(8,128)(2,1)S(1)}, u32[]{:S(2)}, u32[]{:S(2)}) %collective-permute-start.10) | collective-permute-done | bytes 786464 | tf_op jit(solution)/shard_map/ppermute | solution.py:64
  198.3 16.0 %collective-permute-done.23.refs_4_ = bf16[768,512]{1,0:T(8,128)(2,1)} collective-permute-done((bf16[768,512]{1,0:T(8,128)(2,1)S(1)}, bf16[768,512]{1,0:T(8,128)(2,1)}, u32[]{:S(2)}, u32[]{:S(2)}) %collective-permute-start.23) | collective-permute-done | bytes 786464 | tf_op jit(solution)/shard_map/ppermute | solution.py:64
  214.3 6.4 %pick_blocks.1 = bf16[768,2048]{1,0:T(8,128)(2,1)} custom-call(s32[16]{0:T(128)} %stack.169.refs_0_, bf16[768,512]{1,0:T(8,128)(2,1)} %pad_maximum_fusion.2.refs_1_.refs_0_, bf16[768,512]{1,0:T(8,128)(2,1)} %copy-done.13, bf16[768,512]{1,0:T(8,128)(2,1)} %copy-done.12, bf16[768,512]{1,0:T(8,128)(2,1)} %collective-permute-done.23.refs_4_), custom_call_target="tpu_custom_call" | custom-call | tf_op jit(solution)/shard_map/pick_blocks/pallas_call | solution.py:229
  220.7 4.0 %fusion.6 = f32[768,1024]{1,0:T(8,128)S(1)} fusion(bf16[1024,1024]{1,0:T(8,128)(2,1)} %collective-permute-done.28, bf16[768,2048]{1,0:T(8,128)(2,1)} %pick_blocks.1), kind=kOutput, calls=%fused_computation.14 | convolution fusion | flops 1610612736 | bytes 6815744 | tf_op jit(solution)/shard_map/dot_general | solution.py:245
  224.8 2.9 %add_convert_fusion = bf16[768,1024]{1,0:T(8,128)(2,1)} fusion(f32[768,1024]{1,0:T(8,128)S(1)} %fusion.6, bf16[1024,1024]{1,0:T(8,128)(2,1)S(1)} %copy-done.6, bf16[768,2048]{1,0:T(8,128)(2,1)S(1)} %copy-done.3), kind=kOutput, calls=%fused_computation.12 | convolution fusion | flops 1612185600 | bytes 8388608 | tf_op jit(solution)/shard_map/dot_general | solution.py:245
  (149 shorter events, 19.1 us)
Async XLA Ops:
  0.0 26.3 %copy-start.9 = (bf16[768,1024]{1,0:T(8,128)(2,1)S(1)}, bf16[768,1024]{1,0:T(8,128)(2,1)}, u32[]{:S(2)}) copy-start(bf16[768,1024]{1,0:T(8,128)(2,1)} %refs_2_.1) | copy-start | bytes 4718596
  0.0 27.8 %copy-start.20 = (bf16[256,512]{1,0:T(8,128)(2,1)S(1)}, bf16[256,512]{1,0:T(8,128)(2,1)}, u32[]{:S(2)}) copy-start(bf16[256,512]{1,0:T(8,128)(2,1)} %param.19) | copy-start | bytes 786436
  0.0 27.8 %copy-start.21 = (bf16[256,512]{1,0:T(8,128)(2,1)S(1)}, bf16[256,512]{1,0:T(8,128)(2,1)}, u32[]{:S(2)}) copy-start(bf16[256,512]{1,0:T(8,128)(2,1)} %param.21) | copy-start | bytes 786436
  2.9 37.4 %copy-start.8 = (bf16[256,768]{1,0:T(8,128)(2,1)}, bf16[256,768]{1,0:T(8,128)(2,1)S(1)}, u32[]{:S(2)}) copy-start(bf16[256,768]{1,0:T(8,128)(2,1)S(1)} %constant_dynamic-update-slice_fusion.refs_0_) | copy-start | bytes 1179652
  2.9 11.0 %collective-permute-start.1 = (bf16[128,768]{1,0:T(8,128)(2,1)S(1)}, bf16[128,768]{1,0:T(8,128)(2,1)S(1)}, u32[]{:S(2)}, u32[]{:S(2)}) collective-permute-start(bf16[128,768]{1,0:T(8,128)(2,1)S(1)} %constant_dynamic-slice_fusion.3), channel_id=1, source_target_pairs={{0,4},{2,6},{4,8},{6,10},{8,12},{10,14},{12,0},{14,2},{1,5},{3,7},... | collective-permute-start | bytes 589832 | tf_op jit(solution)/shard_map/ppermute | solution.py:71
  6.0 15.5 %collective-permute-start.2 = (bf16[128,768]{1,0:T(8,128)(2,1)S(1)}, bf16[128,768]{1,0:T(8,128)(2,1)S(1)}, u32[]{:S(2)}, u32[]{:S(2)}) collective-permute-start(bf16[128,768]{1,0:T(8,128)(2,1)S(1)} %constant_dynamic-slice_fusion.3), channel_id=1, source_target_pairs={{0,8},{2,10},{4,12},{6,14},{8,0},{10,2},{12,4},{14,6},{1,9},{3,11}... | collective-permute-start | bytes 589832 | tf_op jit(solution)/shard_map/ppermute | solution.py:71
  8.6 12.9 %collective-permute-start.3 = (bf16[128,768]{1,0:T(8,128)(2,1)S(1)}, bf16[128,768]{1,0:T(8,128)(2,1)S(1)}, u32[]{:S(2)}, u32[]{:S(2)}) collective-permute-start(bf16[128,768]{1,0:T(8,128)(2,1)S(1)} %constant_dynamic-slice_fusion.3), channel_id=1, source_target_pairs={{0,12},{2,14},{4,0},{6,2},{8,4},{10,6},{12,8},{14,10},{1,13},{3,15... | collective-permute-start | bytes 589832 | tf_op jit(solution)/shard_map/ppermute | solution.py:71
  13.9 7.6 %copy-start.25 = (bf16[128,768]{1,0:T(8,128)(2,1)}, bf16[128,768]{1,0:T(8,128)(2,1)S(1)}, u32[]{:S(2)}) copy-start(bf16[128,768]{1,0:T(8,128)(2,1)S(1)} %collective-permute-done.1.refs_0_) | copy-start | bytes 589828
  21.5 0.7 copy-start.26
  24.8 15.5 %collective-permute-start.4 = (bf16[384,768]{1,0:T(8,128)(2,1)}, bf16[384,768]{1,0:T(8,128)(2,1)}, u32[]{:S(2)}, u32[]{:S(2)}) collective-permute-start(bf16[384,768]{1,0:T(8,128)(2,1)} %join_rows.8.refs_1_), channel_id=1, source_target_pairs={{0,16},{16,0},{1,17},{17,1},{2,18},{18,2},{3,19},{19,3},{4,20},{20... | collective-permute-start | bytes 1769480 | tf_op jit(solution)/shard_map/ppermute | solution.py:64
  26.3 36.0 %collective-permute-start = (bf16[768,1024]{1,0:T(8,128)(2,1)S(1)}, bf16[768,1024]{1,0:T(8,128)(2,1)}, u32[]{:S(2)}, u32[]{:S(2)}) collective-permute-start(bf16[768,1024]{1,0:T(8,128)(2,1)S(1)} %copy-done.9), channel_id=1, source_target_pairs={{0,1},{1,0},{2,3},{3,2},{4,5},{5,4},{6,7},{7,6},{8,9},{9,8},{10,11... | collective-permute-start | bytes 4718600 | tf_op jit(solution)/shard_map/ppermute | solution.py:64
  27.9 15.1 %copy-start.32 = (s32[768]{0:T(1024)S(1)}, s32[768]{0:T(1024)}, u32[]{:S(2)}) copy-start(s32[768]{0:T(1024)} %param.27) | copy-start | bytes 9220
  27.9 15.1 %copy-start.15 = (bf16[256,512]{1,0:T(8,128)(2,1)S(1)}, bf16[256,512]{1,0:T(8,128)(2,1)}, u32[]{:S(2)}) copy-start(bf16[256,512]{1,0:T(8,128)(2,1)} %refs_1_.1) | copy-start | bytes 786436
  27.9 15.8 %copy-start.4 = (bf16[256,1024]{1,0:T(8,128)(2,1)}, bf16[256,1024]{1,0:T(8,128)(2,1)S(1)}, u32[]{:S(2)}) copy-start(bf16[256,1024]{1,0:T(8,128)(2,1)S(1)} %constant_dynamic-update-slice_fusion.3.refs_1_) | copy-start | bytes 1572868
  27.9 15.8 %copy-start.22 = (bf16[128,1024]{1,0:T(8,128)(2,1)S(1)}, bf16[128,1024]{1,0:T(8,128)(2,1)}, u32[]{:S(2)}) copy-start(bf16[128,1024]{1,0:T(8,128)(2,1)} %param.22) | copy-start | bytes 786436
  28.0 20.4 %collective-permute-start.16 = (bf16[128,1024]{1,0:T(8,128)(2,1)S(1)}, bf16[128,1024]{1,0:T(8,128)(2,1)}, u32[]{:S(2)}, u32[]{:S(2)}) collective-permute-start(bf16[128,1024]{1,0:T(8,128)(2,1)S(1)} %constant_dynamic-slice_fusion.1), channel_id=1, source_target_pairs={{0,4},{2,6},{4,8},{6,10},{8,12},{10,14},{12,0},{14,2},{1,5},{3,7},... | collective-permute-start | bytes 786440 | tf_op jit(solution)/shard_map/ppermute | solution.py:71
  32.0 20.5 %collective-permute-start.17 = (bf16[128,1024]{1,0:T(8,128)(2,1)S(1)}, bf16[128,1024]{1,0:T(8,128)(2,1)}, u32[]{:S(2)}, u32[]{:S(2)}) collective-permute-start(bf16[128,1024]{1,0:T(8,128)(2,1)S(1)} %constant_dynamic-slice_fusion.1), channel_id=1, source_target_pairs={{0,8},{2,10},{4,12},{6,14},{8,0},{10,2},{12,4},{14,6},{1,9},{3,11}... | collective-permute-start | bytes 786440 | tf_op jit(solution)/shard_map/ppermute | solution.py:71
  34.3 19.5 %collective-permute-start.18 = (bf16[128,1024]{1,0:T(8,128)(2,1)S(1)}, bf16[128,1024]{1,0:T(8,128)(2,1)}, u32[]{:S(2)}, u32[]{:S(2)}) collective-permute-start(bf16[128,1024]{1,0:T(8,128)(2,1)S(1)} %constant_dynamic-slice_fusion.1), channel_id=1, source_target_pairs={{0,12},{2,14},{4,0},{6,2},{8,4},{10,6},{12,8},{14,10},{1,13},{3,15... | collective-permute-start | bytes 786440 | tf_op jit(solution)/shard_map/ppermute | solution.py:71
  42.9 29.7 %collective-permute-start.5 = (bf16[1024,768]{1,0:T(8,128)(2,1)}, bf16[1024,768]{1,0:T(8,128)(2,1)}, u32[]{:S(2)}, u32[]{:S(2)}) collective-permute-start(bf16[1024,768]{1,0:T(8,128)(2,1)} %join_rows.9), channel_id=1, source_target_pairs={{0,2},{2,0},{4,6},{6,4},{8,10},{10,8},{12,14},{14,12},{1,3},{3,1},... | collective-permute-start | bytes 4718600 | tf_op jit(solution)/shard_map/ppermute | solution.py:119
  44.7 52.1 %copy-start.5 = (bf16[256,1024]{1,0:T(8,128)(2,1)}, bf16[256,1024]{1,0:T(8,128)(2,1)S(1)}, u32[]{:S(2)}) copy-start(bf16[256,1024]{1,0:T(8,128)(2,1)S(1)} %constant_dynamic-update-slice_fusion.5.refs_1_) | copy-start | bytes 1572868
  48.4 52.4 %collective-permute-start.11 = (bf16[128,512]{1,0:T(8,128)(2,1)}, bf16[128,512]{1,0:T(8,128)(2,1)}, u32[]{:S(2)}, u32[]{:S(2)}) collective-permute-start(bf16[128,512]{1,0:T(8,128)(2,1)} %constant_dynamic-slice_fusion.2), channel_id=1, source_target_pairs={{0,4},{2,6},{4,8},{6,10},{8,12},{10,14},{12,0},{14,2},{1,5},{3,7},... | collective-permute-start | bytes 393224 | tf_op jit(solution)/shard_map/ppermute | solution.py:71
  52.6 50.3 %collective-permute-start.12 = (bf16[128,512]{1,0:T(8,128)(2,1)}, bf16[128,512]{1,0:T(8,128)(2,1)}, u32[]{:S(2)}, u32[]{:S(2)}) collective-permute-start(bf16[128,512]{1,0:T(8,128)(2,1)} %constant_dynamic-slice_fusion.2), channel_id=1, source_target_pairs={{0,8},{2,10},{4,12},{6,14},{8,0},{10,2},{12,4},{14,6},{1,9},{3,11}... | collective-permute-start | bytes 393224 | tf_op jit(solution)/shard_map/ppermute | solution.py:71
  53.8 43.1 %collective-permute-start.8 = (bf16[1,128]{1,0:T(2,128)(2,1)}, bf16[1,128]{1,0:T(2,128)(2,1)S(1)}, u32[]{:S(2)}, u32[]{:S(2)}) collective-permute-start(bf16[1,128]{1,0:T(2,128)(2,1)} %get-tuple-element.54), channel_id=1, source_target_pairs={{2,0},{4,2},{6,4},{8,6},{10,8},{12,10},{14,12},{3,1},{5,3},{7,5},{... | collective-permute-start | bytes 776 | tf_op jit(solution)/shard_map/ppermute | solution.py:26
  57.2 15.4 %copy-start.2 = (bf16[384,1024]{1,0:T(8,128)(2,1)S(1)}, bf16[384,1024]{1,0:T(8,128)(2,1)}, u32[]{:S(2)}) copy-start(bf16[384,1024]{1,0:T(8,128)(2,1)} %join_rows.12.refs_2_) | copy-start | bytes 2359300
  62.4 36.4 %collective-permute-start.7 = (bf16[1,128]{1,0:T(2,128)(2,1)}, bf16[1,128]{1,0:T(2,128)(2,1)S(1)}, u32[]{:S(2)}, u32[]{:S(2)}) collective-permute-start(bf16[1,128]{1,0:T(2,128)(2,1)} %get-tuple-element.53), channel_id=1, source_target_pairs={{0,2},{2,4},{4,6},{6,8},{8,10},{10,12},{12,14},{1,3},{3,5},{5,7},{... | collective-permute-start | bytes 776 | tf_op jit(solution)/shard_map/ppermute | solution.py:24
  72.6 16.6 %collective-permute-start.19 = (bf16[384,1024]{1,0:T(8,128)(2,1)S(1)}, bf16[384,1024]{1,0:T(8,128)(2,1)S(1)}, u32[]{:S(2)}, u32[]{:S(2)}) collective-permute-start(bf16[384,1024]{1,0:T(8,128)(2,1)S(1)} %copy-done.2), channel_id=1, source_target_pairs={{0,16},{16,0},{1,17},{17,1},{2,18},{18,2},{3,19},{19,3},{4,20},{20... | collective-permute-start | bytes 2359304 | tf_op jit(solution)/shard_map/ppermute | solution.py:64
  73.1 3.4 %copy-start.10 = (bf16[1024,768]{1,0:T(8,128)(2,1)S(1)}, bf16[1024,768]{1,0:T(8,128)(2,1)}, u32[]{:S(2)}) copy-start(bf16[1024,768]{1,0:T(8,128)(2,1)} %join_rows.9) | copy-start | bytes 4718596
  73.1 3.4 %copy-start.33 = (bf16[768,2048]{1,0:T(8,128)(2,1)S(1)}, bf16[768,2048]{1,0:T(8,128)(2,1)}, u32[]{:S(2)}) copy-start(bf16[768,2048]{1,0:T(8,128)(2,1)} %get-tuple-element.7) | copy-start | bytes 9437188
  78.0 1.4 copy-start.23
  80.6 16.1 %copy-start.31 = (f32[3,512]{1,0:T(4,128)S(1)}, f32[3,512]{1,0:T(4,128)}, u32[]{:S(2)}) copy-start(f32[3,512]{1,0:T(4,128)} %param.25) | copy-start | bytes 18436
  80.6 16.2 %copy-start.36 = (f32[8]{0:T(128)S(1)}, f32[8]{0:T(128)}, u32[]{:S(2)}) copy-start(f32[8]{0:T(128)} %param.24) | copy-start | bytes 100
  89.1 0.9 copy-start.14
  93.0 42.6 %collective-permute-start.20 = (bf16[1024,1024]{1,0:T(8,128)(2,1)}, bf16[1024,1024]{1,0:T(8,128)(2,1)}, u32[]{:S(2)}, u32[]{:S(2)}) collective-permute-start(bf16[1024,1024]{1,0:T(8,128)(2,1)} %join_rows.13), channel_id=1, source_target_pairs={{0,2},{2,0},{4,6},{6,4},{8,10},{10,8},{12,14},{14,12},{1,3},{3,1},... | collective-permute-start | bytes 6291464 | tf_op jit(solution)/shard_map/ppermute | solution.py:119
  96.9 8.7 %collective-permute-start.13 = (bf16[128,512]{1,0:T(8,128)(2,1)}, bf16[128,512]{1,0:T(8,128)(2,1)S(1)}, u32[]{:S(2)}, u32[]{:S(2)}) collective-permute-start(bf16[128,512]{1,0:T(8,128)(2,1)} %constant_dynamic-slice_fusion.2), channel_id=1, source_target_pairs={{0,12},{2,14},{4,0},{6,2},{8,4},{10,6},{12,8},{14,10},{1,13},{3,15... | collective-permute-start | bytes 393224 | tf_op jit(solution)/shard_map/ppermute | solution.py:71
  98.7 13.8 %collective-permute-start.24 = (bf16[128,1024]{1,0:T(8,128)(2,1)S(1)}, bf16[128,1024]{1,0:T(8,128)(2,1)S(1)}, u32[]{:S(2)}, u32[]{:S(2)}) collective-permute-start(bf16[128,1024]{1,0:T(8,128)(2,1)S(1)} %constant_dynamic-slice_fusion), channel_id=1, source_target_pairs={{0,4},{2,6},{4,8},{6,10},{8,12},{10,14},{12,0},{14,2},{1,5},{3,7},... | collective-permute-start | bytes 786440 | tf_op jit(solution)/shard_map/ppermute | solution.py:71
  100.8 22.8 %collective-permute-start.25 = (bf16[128,1024]{1,0:T(8,128)(2,1)S(1)}, bf16[128,1024]{1,0:T(8,128)(2,1)S(1)}, u32[]{:S(2)}, u32[]{:S(2)}) collective-permute-start(bf16[128,1024]{1,0:T(8,128)(2,1)S(1)} %constant_dynamic-slice_fusion), channel_id=1, source_target_pairs={{0,8},{2,10},{4,12},{6,14},{8,0},{10,2},{12,4},{14,6},{1,9},{3,11}... | collective-permute-start | bytes 786440 | tf_op jit(solution)/shard_map/ppermute | solution.py:71
  102.9 26.3 %collective-permute-start.26 = (bf16[128,1024]{1,0:T(8,128)(2,1)S(1)}, bf16[128,1024]{1,0:T(8,128)(2,1)S(1)}, u32[]{:S(2)}, u32[]{:S(2)}) collective-permute-start(bf16[128,1024]{1,0:T(8,128)(2,1)S(1)} %constant_dynamic-slice_fusion), channel_id=1, source_target_pairs={{0,12},{2,14},{4,0},{6,2},{8,4},{10,6},{12,8},{14,10},{1,13},{3,15... | collective-permute-start | bytes 786440 | tf_op jit(solution)/shard_map/ppermute | solution.py:71
  108.1 10.6 %collective-permute-start.14 = (bf16[384,512]{1,0:T(8,128)(2,1)}, bf16[384,512]{1,0:T(8,128)(2,1)S(1)}, u32[]{:S(2)}, u32[]{:S(2)}) collective-permute-start(bf16[384,512]{1,0:T(8,128)(2,1)} %join_rows.10.refs_2_), channel_id=1, source_target_pairs={{0,16},{16,0},{1,17},{17,1},{2,18},{18,2},{3,19},{19,3},{4,20},{20... | collective-permute-start | bytes 1179656 | tf_op jit(solution)/shard_map/ppermute | solution.py:64
  112.5 16.7 %copy-start.17 = (bf16[128,1024]{1,0:T(8,128)(2,1)}, bf16[128,1024]{1,0:T(8,128)(2,1)S(1)}, u32[]{:S(2)}) copy-start(bf16[128,1024]{1,0:T(8,128)(2,1)S(1)} %collective-permute-done.24.refs_1_) | copy-start | bytes 786436
  112.5 21.1 %collective-permute-start.6 = (bf16[128,256]{1,0:T(8,128)(2,1)S(1)}, bf16[128,256]{1,0:T(8,128)(2,1)S(1)}, u32[]{:S(2)}, u32[]{:S(2)}) collective-permute-start(bf16[128,256]{1,0:T(8,128)(2,1)S(1)} %get-tuple-element.32), channel_id=1, source_target_pairs={{0,2},{2,4},{4,6},{6,8},{8,10},{10,12},{12,14},{1,3},{3,5},{5,7},{... | collective-permute-start | bytes 196616 | tf_op jit(solution)/shard_map/ppermute | solution.py:24
  118.7 1.6 copy-start.16
  118.7 14.9 %collective-permute-start.9 = (bf16[128,256]{1,0:T(8,128)(2,1)S(1)}, bf16[128,256]{1,0:T(8,128)(2,1)S(1)}, u32[]{:S(2)}, u32[]{:S(2)}) collective-permute-start(bf16[128,256]{1,0:T(8,128)(2,1)S(1)} %get-tuple-element.33), channel_id=1, source_target_pairs={{2,0},{4,2},{6,4},{8,6},{10,8},{12,10},{14,12},{3,1},{5,3},{7,5},{... | collective-permute-start | bytes 196616 | tf_op jit(solution)/shard_map/ppermute | solution.py:26
  123.6 5.6 %copy-start.18 = (bf16[128,1024]{1,0:T(8,128)(2,1)}, bf16[128,1024]{1,0:T(8,128)(2,1)S(1)}, u32[]{:S(2)}) copy-start(bf16[128,1024]{1,0:T(8,128)(2,1)S(1)} %collective-permute-done.25.refs_2_) | copy-start | bytes 786436
  123.6 22.8 %collective-permute-start.15 = (bf16[1024,512]{1,0:T(8,128)(2,1)}, bf16[1024,512]{1,0:T(8,128)(2,1)}, u32[]{:S(2)}, u32[]{:S(2)}) collective-permute-start(bf16[1024,512]{1,0:T(8,128)(2,1)} %join_rows.11), channel_id=1, source_target_pairs={{0,2},{2,0},{4,6},{6,4},{8,10},{10,8},{12,14},{14,12},{1,3},{3,1},... | collective-permute-start | bytes 3145736 | tf_op jit(solution)/shard_map/ppermute | solution.py:119
  129.2 0.7 copy-start.19
  131.9 39.8 %collective-permute-start.27 = (bf16[384,1024]{1,0:T(8,128)(2,1)}, bf16[384,1024]{1,0:T(8,128)(2,1)}, u32[]{:S(2)}, u32[]{:S(2)}) collective-permute-start(bf16[384,1024]{1,0:T(8,128)(2,1)} %join_rows.14.refs_2_), channel_id=1, source_target_pairs={{0,16},{16,0},{1,17},{17,1},{2,18},{18,2},{3,19},{19,3},{4,20},{20... | collective-permute-start | bytes 2359304 | tf_op jit(solution)/shard_map/ppermute | solution.py:64
  135.6 4.0 %copy-start.7 = (bf16[1024,1024]{1,0:T(8,128)(2,1)S(1)}, bf16[1024,1024]{1,0:T(8,128)(2,1)}, u32[]{:S(2)}) copy-start(bf16[1024,1024]{1,0:T(8,128)(2,1)} %join_rows.13) | copy-start | bytes 6291460
  135.6 4.0 %copy-start.34 = (bf16[768,2048]{1,0:T(8,128)(2,1)S(1)}, bf16[768,2048]{1,0:T(8,128)(2,1)}, u32[]{:S(2)}) copy-start(bf16[768,2048]{1,0:T(8,128)(2,1)} %get-tuple-element.7) | copy-start | bytes 9437188
  141.8 6.9 %collective-permute-start.22 = (bf16[1,512]{1,0:T(2,128)(2,1)S(1)}, bf16[1,512]{1,0:T(2,128)(2,1)S(1)}, u32[]{:S(2)}, u32[]{:S(2)}) collective-permute-start(bf16[1,512]{1,0:T(2,128)(2,1)S(1)} %get-tuple-element.19), channel_id=1, source_target_pairs={{2,0},{4,2},{6,4},{8,6},{10,8},{12,10},{14,12},{3,1},{5,3},{7,5},{... | collective-permute-start | bytes 3080 | tf_op jit(solution)/shard_map/ppermute | solution.py:26
  143.1 5.6 %copy-start.11 = (bf16[1024,512]{1,0:T(8,128)(2,1)S(1)}, bf16[1024,512]{1,0:T(8,128)(2,1)}, u32[]{:S(2)}) copy-start(bf16[1024,512]{1,0:T(8,128)(2,1)} %join_rows.11) | copy-start | bytes 3145732
  143.1 5.6 %copy-start.24 = (f32[768,768]{1,0:T(8,128)S(1)}, f32[768,768]{1,0:T(8,128)}, u32[]{:S(2)}) copy-start(f32[768,768]{1,0:T(8,128)} %copy-done.23) | copy-start | bytes 7077892
  143.1 5.6 %copy-start.35 = (f32[512]{0:T(512)S(1)}, f32[512]{0:T(512)}, u32[]{:S(2)}) copy-start(f32[512]{0:T(512)} %param.26) | copy-start | bytes 6148
  143.1 5.5 %collective-permute-start.21 = (bf16[1,512]{1,0:T(2,128)(2,1)S(1)}, bf16[1,512]{1,0:T(2,128)(2,1)S(1)}, u32[]{:S(2)}, u32[]{:S(2)}) collective-permute-start(bf16[1,512]{1,0:T(2,128)(2,1)S(1)} %get-tuple-element.18), channel_id=1, source_target_pairs={{0,2},{2,4},{4,6},{6,8},{8,10},{10,12},{12,14},{1,3},{3,5},{5,7},{... | collective-permute-start | bytes 3080 | tf_op jit(solution)/shard_map/ppermute | solution.py:24
  151.9 27.3 %copy-start.12 = (bf16[768,512]{1,0:T(8,128)(2,1)}, bf16[768,512]{1,0:T(8,128)(2,1)S(1)}, u32[]{:S(2)}) copy-start(bf16[768,512]{1,0:T(8,128)(2,1)S(1)} %get-tuple-element.39.refs_3_) | copy-start | bytes 2359300
  155.8 3.1 %copy-start = (f32[2,640,384,4]{2,1,3,0:T(8,128)}, f32[2,640,384,4]{2,1,3,0:T(8,128)S(1)}, u32[]{:S(2)}) copy-start(f32[2,640,384,4]{2,1,3,0:T(8,128)S(1)} %get-tuple-element.58) | copy-start | bytes 23592964
  160.3 1.8 copy-start.29
  162.1 3.0 %copy-start.28 = (bf16[640,128]{0,1:T(8,128)(2,1)S(1)}, bf16[640,128]{0,1:T(8,128)(2,1)}, u32[]{:S(2)}) copy-start(bf16[640,128]{0,1:T(8,128)(2,1)} %copy.31) | copy-start | bytes 491524
  171.7 6.1 %copy-start.1 = (bf16[768,512]{1,0:T(8,128)(2,1)S(1)}, bf16[768,512]{1,0:T(8,128)(2,1)}, u32[]{:S(2)}) copy-start(bf16[768,512]{1,0:T(8,128)(2,1)} %pad_maximum_fusion.2.refs_1_.refs_0_) | copy-start | bytes 2359300
  174.8 45.9 %collective-permute-start.28 = (bf16[1024,1024]{1,0:T(8,128)(2,1)}, bf16[1024,1024]{1,0:T(8,128)(2,1)}, u32[]{:S(2)}, u32[]{:S(2)}) collective-permute-start(bf16[1024,1024]{1,0:T(8,128)(2,1)} %join_rows.15), channel_id=1, source_target_pairs={{0,2},{2,0},{4,6},{6,4},{8,10},{10,8},{12,14},{14,12},{1,3},{3,1},... | collective-permute-start | bytes 6291464 | tf_op jit(solution)/shard_map/ppermute | solution.py:119
  177.9 20.4 %collective-permute-start.10 = (bf16[768,512]{1,0:T(8,128)(2,1)S(1)}, bf16[768,512]{1,0:T(8,128)(2,1)S(1)}, u32[]{:S(2)}, u32[]{:S(2)}) collective-permute-start(bf16[768,512]{1,0:T(8,128)(2,1)S(1)} %copy-done.1), channel_id=1, source_target_pairs={{0,1},{1,0},{2,3},{3,2},{4,5},{5,4},{6,7},{7,6},{8,9},{9,8},{10,11... | collective-permute-start | bytes 2359304 | tf_op jit(solution)/shard_map/ppermute | solution.py:64
  179.3 35.0 %collective-permute-start.23 = (bf16[768,512]{1,0:T(8,128)(2,1)S(1)}, bf16[768,512]{1,0:T(8,128)(2,1)}, u32[]{:S(2)}, u32[]{:S(2)}) collective-permute-start(bf16[768,512]{1,0:T(8,128)(2,1)S(1)} %get-tuple-element.39.refs_3_), channel_id=1, source_target_pairs={{0,1},{1,0},{2,3},{3,2},{4,5},{5,4},{6,7},{7,6},{8,9},{9,8},{10,11... | collective-permute-start | bytes 2359304 | tf_op jit(solution)/shard_map/ppermute | solution.py:64
  198.3 16.0 %copy-start.13 = (bf16[768,512]{1,0:T(8,128)(2,1)}, bf16[768,512]{1,0:T(8,128)(2,1)S(1)}, u32[]{:S(2)}) copy-start(bf16[768,512]{1,0:T(8,128)(2,1)S(1)} %collective-permute-done.10.refs_2_) | copy-start | bytes 2359300
  220.7 4.0 %copy-start.3 = (bf16[768,2048]{1,0:T(8,128)(2,1)S(1)}, bf16[768,2048]{1,0:T(8,128)(2,1)}, u32[]{:S(2)}) copy-start(bf16[768,2048]{1,0:T(8,128)(2,1)} %pick_blocks.1) | copy-start | bytes 9437188
  220.7 4.0 %copy-start.6 = (bf16[1024,1024]{1,0:T(8,128)(2,1)S(1)}, bf16[1024,1024]{1,0:T(8,128)(2,1)}, u32[]{:S(2)}) copy-start(bf16[1024,1024]{1,0:T(8,128)(2,1)} %join_rows.15) | copy-start | bytes 6291460
  (2 other events, 1.3 us)
